TPU v7x, 256 devices: a whole 4x4x8 slice. The times are simulated.
256 devices in a mesh: ep: 16 (over y, x), tp: 16 (over z, core).
Axes of the slice: x: 4, y: 4, z: 8, core: 2. Of those that a mesh axis runs over, the one named last changes fastest.
Arguments:
- tokens: bfloat16 [256, 4096], P(None, 'ep'), may hold values from -60 to 60
- gain_attn: bfloat16 [4096], P('ep'), may hold values from 0.099609375 to 1.8984375
- w_query: bfloat16 [4096, 2048], P('ep', 'tp'), may hold values from -0.09375 to 0.09375
- w_key: bfloat16 [4096, 2048], P('ep', 'tp'), may hold values from -0.09375 to 0.09375
- w_value: bfloat16 [4096, 2048], P('ep', 'tp'), may hold values from -0.09375 to 0.09375
- w_output: bfloat16 [2048, 4096], P('tp', 'ep'), may hold values from -0.125 to 0.125
- key_cache: bfloat16 [256, 1024, 2048], P('ep', None, 'tp'), may hold values from -6 to 6
- value_cache: bfloat16 [256, 1024, 2048], P('ep', None, 'tp'), may hold values from -10 to 10
- lengths: int32 [256], P('ep'), may hold values from 128 to 1024
- score_shift: float32 [16], P('tp'), may hold values from -9.5 to -3.5
- gain_ffn: bfloat16 [4096], replicated, may hold values from 0.099609375 to 1.8984375
- w_mix: bfloat16 [4096], P('ep'), may hold values from -0.09375 to 0.09375
- w_dense_gate: bfloat16 [4096, 4096], P('ep', 'tp'), may hold values from -0.09375 to 0.09375
- w_dense_up: bfloat16 [4096, 4096], P('ep', 'tp'), may hold values from -0.09375 to 0.09375
- w_dense_down: bfloat16 [4096, 4096], P('tp', 'ep'), may hold values from -0.09375 to 0.09375
- route_group: int32 [256], replicated, may hold values from 0 to 3, as said below
- route_inner: int32 [256, 2], replicated, may hold values from 0 to 3, as said below
- route_weight: float32 [256, 2], replicated, may hold values from 0.3 to 1
- w_exp_gate: bfloat16 [16, 4096, 2048], P('ep', None, 'tp'), may hold values from -0.09375 to 0.09375
- w_exp_up: bfloat16 [16, 4096, 2048], P('ep', None, 'tp'), may hold values from -0.09375 to 0.09375
- w_exp_down: bfloat16 [16, 2048, 4096], P('ep', 'tp'), may hold values from -0.125 to 0.125
Outputs:
- mixed: bfloat16 [256, 4096], P(None, 'ep')
- new_keys: bfloat16 [256, 2048], P('ep', 'tp')
- new_values: bfloat16 [256, 2048], P('ep', 'tp')
Inputs may be any that keep to these rules, and one draw needn't show every extreme that they name: `route_group`: within every aligned block of 16 sequences (the sequences of one index of ep) exactly half of the tokens use one group, the same group in every block; the other groups share the rest. A token's 2 experts inside its group differ. Within every aligned block of 16 sequences no expert (route_group * 4 + route_inner) is used by more than 4 tokens, and the experts of the group that half of the block uses are each used by exactly 4.
All inputs are finite; a program needn't handle non-finite values.
Results may differ from a plain program's by a relative error of at most 0.0039.
The roundings to bfloat16 on the way count: a program that leaves them out, or rounds other values in their place, can miss the bound.
Values may be sent and summed in bfloat16 or wider, within the bound.
A program may use at most 64 MiB of HBM per device.

v0:
```python
import math

import jax
import jax.numpy as jnp
from jax import lax
from jax.sharding import PartitionSpec as P

D = 4096
HD = 128
EPG = 4
TOPK = 2
EXPERTS = 16
CAP = 4


norm_eps = 1e-06


def in_blocks(value, dim, devices):
    before, after = (value.shape[:dim], value.shape[dim + 1 :])
    return jnp.moveaxis(value.reshape(*before, devices, -1, *after), dim, 0)


def summed_on_arrival(value, axis, dim):
    tiles = in_blocks(value, dim, lax.axis_size(axis))
    arrived = lax.all_to_all(tiles, axis, split_axis=0, concat_axis=0, tiled=True)
    return arrived.sum(axis=0)


def sent_to_all(value, axis):
    devices = lax.axis_size(axis)
    return lax.all_to_all(
        jnp.broadcast_to(value[None], (devices, *value.shape)), axis, 0, 0, tiled=True
    )


def joined_along(tiles, dim):
    tiles = jnp.moveaxis(tiles, 0, dim)
    lengths = tiles.shape
    return tiles.reshape(*lengths[:dim], lengths[dim] * lengths[dim + 1], *lengths[dim + 2 :])


def collect(value, axis, dim):
    tiles = sent_to_all(value, axis)
    return joined_along(tiles, dim)


def rows_for(lines, devices):
    spare = -lines.shape[0] % devices
    if not spare:
        return lines
    return jnp.concatenate([lines, jnp.zeros((spare, *lines.shape[1:]), lines.dtype)])


def nested_sum(value, axes):
    lines = value.reshape(-1, value.shape[-1])
    own = summed_on_arrival(rows_for(lines, lax.axis_size(axes)), axes, 0)
    whole = collect(own, axes, 0)
    return whole[: len(lines)].reshape(value.shape)


def sum_by_parts(value, axes):
    padded = rows_for(value, lax.axis_size(axes))
    whole = collect(summed_on_arrival(padded, axes, 0), axes, 0)
    return lax.slice_in_dim(whole, 0, len(value)).reshape(value.shape)


def packed_total(arrays, axis):
    ravelled, at, outs = (jnp.concatenate([a.reshape(-1) for a in arrays]), 0, [])
    total = sum_by_parts(ravelled, axis)
    for a in arrays:
        outs.append(total[at : at + a.size].reshape(a.shape))
        at += a.size
    return tuple(outs)


def on_device(
    tokens,
    gain_attn,
    w_query,
    w_key,
    w_value,
    w_output,
    key_cache,
    value_cache,
    lengths,
    score_shift,
    gain_ffn,
    w_mix,
    w_dense_gate,
    w_dense_up,
    w_dense_down,
    route_group,
    route_inner,
    route_weight,
    w_exp_gate,
    w_exp_up,
    w_exp_down,
):
    ep_count = lax.axis_size("ep")
    batch_all, col_width = tokens.shape
    seq_local = batch_all // ep_count
    head_cols = w_query.shape[1]
    heads_local = head_cols // HD
    tokens_float = tokens.astype(jnp.float32)
    squares = summed_on_arrival(jnp.sum(tokens_float * tokens_float, axis=1), "ep", 0)
    inv_first = lax.rsqrt(squares / D + norm_eps)[:, None]
    scaled_in = (tokens_float * gain_attn.astype(jnp.float32)).astype(jnp.bfloat16)
    w_joint = jnp.concatenate([w_query, w_key, w_value], axis=1)
    joint_proj = (
        summed_on_arrival(jnp.dot(scaled_in, w_joint, preferred_element_type=jnp.float32), "ep", 0)
        * inv_first
    )
    queries = joint_proj[:, :head_cols].astype(jnp.bfloat16)
    new_keys = joint_proj[:, head_cols : 2 * head_cols].astype(jnp.bfloat16)
    new_values = joint_proj[:, 2 * head_cols :].astype(jnp.bfloat16)
    cache_len = key_cache.shape[1]
    head_query = queries.reshape(seq_local, heads_local, HD)
    head_keys = key_cache.reshape(seq_local, cache_len, heads_local, HD)
    scores = jnp.einsum(
        "bhd,blhd->bhl", head_query, head_keys, preferred_element_type=jnp.float32
    ) / math.sqrt(HD)
    scores = scores + score_shift[None, :, None]
    live_mask = lax.broadcasted_iota(jnp.int32, scores.shape, 2) < lengths[:, None, None]
    soft_terms = jnp.where(live_mask, jax.nn.softplus(scores), 0.0)
    later_sum = lax.cumsum(soft_terms, axis=2, reverse=True) - soft_terms
    stick = jnp.where(live_mask, jnp.exp(jax.nn.log_sigmoid(scores) - later_sum), 0.0).astype(
        jnp.bfloat16
    )
    head_values = value_cache.reshape(seq_local, cache_len, heads_local, HD)
    attended = jnp.einsum("bhl,blhd->bhd", stick, head_values, preferred_element_type=jnp.float32)
    attended = attended.reshape(seq_local, head_cols).astype(jnp.bfloat16)
    attn_part = jnp.dot(collect(attended, "ep", 0), w_output, preferred_element_type=jnp.float32)
    attn_out = nested_sum(attn_part, "tp")
    middle = (tokens_float + attn_out).astype(jnp.bfloat16)
    middle_float = middle.astype(jnp.float32)
    gain_float = gain_ffn.astype(jnp.float32)
    gain_cols = lax.dynamic_slice_in_dim(gain_float, lax.axis_index("ep") * col_width, col_width, 0)
    scaled_mid = (middle_float * gain_cols).astype(jnp.bfloat16)
    dense_pre, dense_lin, mix_pre, mid_squares = packed_total(
        (
            jnp.dot(scaled_mid, w_dense_gate, preferred_element_type=jnp.float32),
            jnp.dot(scaled_mid, w_dense_up, preferred_element_type=jnp.float32),
            jnp.dot(scaled_mid, w_mix, preferred_element_type=jnp.float32),
            jnp.sum(middle_float * middle_float, axis=1),
        ),
        "ep",
    )
    inv_second = lax.rsqrt(mid_squares / D + norm_eps)[:, None]
    dense_hidden = (jax.nn.silu(dense_pre * inv_second) * (dense_lin * inv_second)).astype(
        jnp.bfloat16
    )
    mix_gate = jax.nn.sigmoid(mix_pre * inv_second[:, 0])
    dense_part = (
        jnp.dot(dense_hidden, w_dense_down, preferred_element_type=jnp.float32) * mix_gate[:, None]
    )
    slot_count = CAP * ep_count
    expert_ids = (route_group[:, None] * EPG + route_inner).reshape(-1)
    expert_onehot = (expert_ids[:, None] == jnp.arange(EXPERTS, dtype=jnp.int32)[None, :]).astype(
        jnp.int32
    )
    per_block = expert_onehot.reshape(ep_count, seq_local * TOPK, EXPERTS)
    earlier = (jnp.cumsum(per_block, axis=1) - per_block).reshape(-1, EXPERTS)
    slot_rank = jnp.sum(earlier * expert_onehot, axis=1)
    route_index = jnp.arange(batch_all * TOPK, dtype=jnp.int32)
    block_of = route_index // (seq_local * TOPK)
    slot_flat = expert_ids * slot_count + block_of * CAP + slot_rank
    slot_table = (
        jnp.full((EXPERTS * slot_count,), batch_all, jnp.int32)
        .at[slot_flat]
        .set(route_index // TOPK)
    )
    padded_middle = jnp.concatenate([middle, jnp.zeros((1, col_width), jnp.bfloat16)], axis=0)
    outgoing = jnp.take(padded_middle, slot_table, axis=0).reshape(EXPERTS, slot_count, col_width)
    arrived_float = lax.all_to_all(outgoing, "ep", split_axis=0, concat_axis=2, tiled=True).astype(
        jnp.float32
    )
    inv_rows = lax.rsqrt(jnp.mean(arrived_float * arrived_float, axis=2, keepdims=True) + norm_eps)
    scaled_rows = (arrived_float * gain_float).astype(jnp.bfloat16)
    gate_pre = (
        jnp.einsum("end,edf->enf", scaled_rows, w_exp_gate, preferred_element_type=jnp.float32)
        * inv_rows
    )
    up_proj = (
        jnp.einsum("end,edf->enf", scaled_rows, w_exp_up, preferred_element_type=jnp.float32)
        * inv_rows
    )
    hidden = (jax.nn.silu(gate_pre) * up_proj).astype(jnp.bfloat16)
    expert_rows = jnp.einsum("enf,efd->end", hidden, w_exp_down, preferred_element_type=jnp.float32)
    returned = lax.all_to_all(expert_rows, "ep", split_axis=2, concat_axis=0, tiled=True)
    flat_back = returned.reshape(EXPERTS * slot_count, col_width)
    routed = jnp.take(flat_back, slot_flat, axis=0).reshape(batch_all, TOPK, col_width)
    expert_part = jnp.sum(routed * route_weight[:, :, None], axis=1)
    result_sum = middle_float + nested_sum(expert_part + dense_part, "tp")
    return (result_sum.astype(jnp.bfloat16), new_keys, new_values)


def solution(mesh):
    placed = (
        P(None, "ep"),
        P("ep"),
        P("ep", "tp"),
        P("ep", "tp"),
        P("ep", "tp"),
        P("tp", "ep"),
        P("ep", None, "tp"),
        P("ep", None, "tp"),
        P("ep"),
        P("tp"),
        P(),
        P("ep"),
        P("ep", "tp"),
        P("ep", "tp"),
        P("tp", "ep"),
        P(),
        P(),
        P(),
        P("ep", None, "tp"),
        P("ep", None, "tp"),
        P("ep", "tp", None),
    )
    return jax.shard_map(
        on_device,
        mesh=mesh,
        in_specs=placed,
        out_specs=(P(None, "ep"), P("ep", "tp"), P("ep", "tp")),
        check_vma=False,
    )
```

profile of v0, /device:TPU:1, one launch (start us, length us, event | category | flops | bytes accessed | tf_op | source)
XLA Modules:
  0.0 242.0 jit_solution(13241488657580019274)
XLA Ops:
  0.7 1.1 fusion.13
  1.8 0.7 all_to_all.53
  2.5 7.6 %all-to-all-start.1 = ((f32[16,1,16]{2,1,0:T(1,128)}), f32[16,1,16]{2,1,0:T(1,128)S(1)}, u32[]{:S(2)}, u32[]{:S(2)}) async-start(f32[16,1,16]{2,1,0:T(1,128)} %all_to_all.53), calls=%async_computation.1 | async-start | bytes 16384 | tf_op jit(solution)/shard_map/all_to_all | solution.py:26
  10.7 1.9 fusion.21
  12.6 3.8 %all-to-all-done.1 = f32[16,1,16]{2,1,0:T(1,128)S(1)} async-done(((f32[16,1,16]{2,1,0:T(1,128)}), f32[16,1,16]{2,1,0:T(1,128)S(1)}, u32[]{:S(2)}, u32[]{:S(2)}) %all-to-all-start.1) | async-done | bytes 1056 | tf_op jit(solution)/shard_map/all_to_all | solution.py:26
  16.4 3.6 %all-to-all-start = ((f32[16,16,384]{2,1,0:T(8,128)}), f32[16,16,384]{2,1,0:T(8,128)S(1)}, u32[]{:S(2)}, u32[]{:S(2)}) async-start(f32[16,16,384]{2,1,0:T(8,128)} %bitcast), calls=%async_computation | async-start | bytes 786432 | tf_op jit(solution)/shard_map/all_to_all | solution.py:26
  20.6 7.8 %all-to-all-done = f32[16,16,384]{2,1,0:T(8,128)S(1)} async-done(((f32[16,16,384]{2,1,0:T(8,128)}), f32[16,16,384]{2,1,0:T(8,128)S(1)}, u32[]{:S(2)}, u32[]{:S(2)}) %all-to-all-start) | async-done | bytes 393248 | tf_op jit(solution)/shard_map/all_to_all | solution.py:26
  29.1 3.4 %fusion.58 = f32[16,1,1024]{2,1,0:T(1,128)S(1)} fusion(bf16[16,1024,128]{2,1,0:T(8,128)(2,1)} %param.27, bf16[16,128,1]{1,0,2:T(8,128)(2,1)S(1)} %get-tuple-element.13), kind=kOutput, calls=%fused_computation.83 | convolution fusion | flops 4194304 | bytes 4263936 | tf_op jit(solution)/shard_map/bhd,blhd->bhl/dot_general | solution.py:120
  32.7 19.8 %reduce-window.6 = f32[16,1,8,128]{3,2,1,0:T(8,128)S(1)} reduce-window(f32[16,1,8,128]{3,2,1,0:T(8,128)S(1)} %bitcast.112, f32[]{:T(128)} %constant.93.clone.1), window={size=1x1x1x128 pad=0_0x0_0x0_0x0_127}, to_apply=%region_3.4 | reduce-window | flops 2080768 | bytes 131076 | tf_op jit(solution)/shard_map/reduce-window
  52.9 2.8 %fusion.47 = f32[16,1,128]{2,1,0:T(1,128)S(1)} fusion(bf16[16,1024,128]{2,1,0:T(8,128)(2,1)} %param.28, bf16[16,1024,1]{1,0,2:T(8,128)(2,1)S(1)} %fusion.55), kind=kOutput, calls=%fused_computation.68 | convolution fusion | flops 4194304 | bytes 4235264 | tf_op jit(solution)/shard_map/bhl,blhd->bhd/dot_general | solution.py:131
  56.4 3.5 %all-to-all-start.2 = ((bf16[16,16,128]{2,1,0:T(8,128)(2,1)}), bf16[16,16,128]{2,1,0:T(8,128)(2,1)S(1)}, u32[]{:S(2)}, u32[]{:S(2)}) async-start(bf16[16,16,128]{2,1,0:T(8,128)(2,1)} %broadcast_in_dim.34), calls=%async_computation.2 | async-start | bytes 131072 | tf_op jit(solution)/shard_map/all_to_all | solution.py:32
  60.0 6.4 %all-to-all-done.2 = bf16[16,16,128]{2,1,0:T(8,128)(2,1)S(1)} async-done(((bf16[16,16,128]{2,1,0:T(8,128)(2,1)}), bf16[16,16,128]{2,1,0:T(8,128)(2,1)S(1)}, u32[]{:S(2)}, u32[]{:S(2)}) %all-to-all-start.2) | async-done | bytes 65568 | tf_op jit(solution)/shard_map/all_to_all | solution.py:32
  66.4 0.9 fusion.44
  67.3 12.6 %all-to-all-start.3 = ((f32[16,16,256]{2,1,0:T(8,128)}), f32[16,16,256]{2,1,0:T(8,128)S(1)}, u32[]{:S(2)}, u32[]{:S(2)}) async-start(f32[16,16,256]{2,1,0:T(8,128)} %fusion.44), calls=%async_computation.3 | async-start | bytes 524288 | tf_op jit(solution)/shard_map/all_to_all | solution.py:26
  80.2 0.8 fusion.80
  81.6 9.9 %all-to-all-done.3 = f32[16,16,256]{2,1,0:T(8,128)S(1)} async-done(((f32[16,16,256]{2,1,0:T(8,128)}), f32[16,16,256]{2,1,0:T(8,128)S(1)}, u32[]{:S(2)}, u32[]{:S(2)}) %all-to-all-start.3) | async-done | bytes 262176 | tf_op jit(solution)/shard_map/all_to_all | solution.py:26
  91.5 0.7 broadcast_in_dim.35
  92.2 3.4 %all-to-all-start.4 = ((f32[16,16,256]{2,1,0:T(8,128)}), f32[16,16,256]{2,1,0:T(8,128)S(1)}, u32[]{:S(2)}, u32[]{:S(2)}) async-start(f32[16,16,256]{2,1,0:T(8,128)} %broadcast_in_dim.35), calls=%async_computation.4 | async-start | bytes 524288 | tf_op jit(solution)/shard_map/all_to_all | solution.py:32
  95.7 2.4 %scatter_custom_fusion = s32[1024]{0:T(1024)S(1)} fusion(s32[512]{0:T(512)S(1)} %bitcast.116, s32[512]{0:T(512)S(1)} %add_select_fusion, s32[]{:T(128)} %constant.107.clone.1), kind=kCustom, calls=%fused_computation.106 | custom fusion | bytes 4100 | tf_op jit(solution)/shard_map/scatter | solution.py:171
  98.3 8.5 %all-to-all-done.4 = f32[16,16,256]{2,1,0:T(8,128)S(1)} async-done(((f32[16,16,256]{2,1,0:T(8,128)}), f32[16,16,256]{2,1,0:T(8,128)S(1)}, u32[]{:S(2)}, u32[]{:S(2)}) %all-to-all-start.4) | async-done | bytes 262176 | tf_op jit(solution)/shard_map/all_to_all | solution.py:32
  107.0 3.9 %gather_fusion = bf16[1024,256]{1,0:T(8,128)(2,1)S(1)} fusion(bf16[257,256]{1,0:T(8,128)(2,1)S(1)} %concatenate.10, s32[1024]{0:T(1024)S(1)} %fusion.60), kind=kCustom, calls=%fused_computation | custom fusion | bytes 1052672 | tf_op jit(solution)/shard_map/jit(_take)/gather | solution.py:174
  110.9 1.0 broadcast_select_fusion
  111.9 3.6 %all-to-all-start.5 = ((bf16[16,64,256]{2,1,0:T(8,128)(2,1)}), bf16[16,64,256]{2,1,0:T(8,128)(2,1)S(1)}, u32[]{:S(2)}, u32[]{:S(2)}) async-start(bf16[16,64,256]{2,1,0:T(8,128)(2,1)} %broadcast_select_fusion), calls=%async_computation.5 | async-start | bytes 1048576 | tf_op jit(solution)/shard_map/all_to_all | solution.py:175
  116.4 1.5 all_to_all.62
  117.9 8.9 %all-to-all-done.5 = bf16[16,64,256]{2,1,0:T(8,128)(2,1)S(1)} async-done(((bf16[16,64,256]{2,1,0:T(8,128)(2,1)}), bf16[16,64,256]{2,1,0:T(8,128)(2,1)S(1)}, u32[]{:S(2)}, u32[]{:S(2)}) %all-to-all-start.5) | async-done | bytes 524320 | tf_op jit(solution)/shard_map/all_to_all | solution.py:175
  126.9 3.6 %all-to-all-start.7 = ((f32[16,1,8224]{2,1,0:T(1,128)}), f32[16,1,8224]{2,1,0:T(1,128)S(1)}, u32[]{:S(2)}, u32[]{:S(2)}) async-start(f32[16,1,8224]{2,1,0:T(1,128)} %all_to_all.62), calls=%async_computation.7 | async-start | bytes 1064960 | tf_op jit(solution)/shard_map/all_to_all | solution.py:26
  130.8 10.3 %all-to-all-done.7 = f32[16,1,8224]{2,1,0:T(1,128)S(1)} async-done(((f32[16,1,8224]{2,1,0:T(1,128)}), f32[16,1,8224]{2,1,0:T(1,128)S(1)}, u32[]{:S(2)}, u32[]{:S(2)}) %all-to-all-start.7) | async-done | bytes 526368 | tf_op jit(solution)/shard_map/all_to_all | solution.py:26
  141.4 1.1 broadcast_in_dim.77
  142.5 4.4 %all-to-all-start.8 = ((f32[16,1,8224]{2,1,0:T(1,128)}), f32[16,1,8224]{2,1,0:T(1,128)}, u32[]{:S(2)}, u32[]{:S(2)}) async-start(f32[16,1,8224]{2,1,0:T(1,128)} %broadcast_in_dim.77), calls=%async_computation.8 | async-start | bytes 1064960 | tf_op jit(solution)/shard_map/all_to_all | solution.py:32
  147.0 1.5 convolution_multiply_fusion.2
  148.5 2.1 fusion.4
  151.2 19.4 %reduce.8 = f32[4096,64]{1,0:T(8,128)} reduce(f32[4096,1,64]{2,1,0:T(1,128)S(1)} %bitcast.100, f32[]{:T(128)} %broadcast.260), dimensions={1}, to_apply=%bitcast.84.reduce_sub_computation | reduce | bytes 2097156
  170.5 3.4 %reshape.403 = f32[16,1,16384]{2,1,0:T(1,128)} reshape(f32[4096,64]{1,0:T(8,128)} %reduce.8) | data formatting | bytes 2097152
  174.0 6.4 %all-to-all-start.6 = ((f32[16,1,16384]{2,1,0:T(1,128)}), f32[16,1,16384]{2,1,0:T(1,128)S(1)}, u32[]{:S(2)}, u32[]{:S(2)}) async-start(f32[16,1,16384]{2,1,0:T(1,128)} %reshape.403), calls=%async_computation.6 | async-start | bytes 2097152 | tf_op jit(solution)/shard_map/all_to_all | solution.py:190
  180.9 2.3 reduce.6
  183.2 1.0 reshape.363
  184.3 1.1 slice.37
  185.3 0.8 fusion.73
  186.1 9.2 %all-to-all-done.6 = f32[16,1,16384]{2,1,0:T(1,128)S(1)} async-done(((f32[16,1,16384]{2,1,0:T(1,128)}), f32[16,1,16384]{2,1,0:T(1,128)S(1)}, u32[]{:S(2)}, u32[]{:S(2)}) %all-to-all-start.6) | async-done | bytes 1048608 | tf_op jit(solution)/shard_map/all_to_all | solution.py:190
  195.3 3.1 %reduce.9 = f32[16,16384]{1,0:T(8,128)S(1)} reduce(f32[16,1,16384]{2,1,0:T(1,128)S(1)} %all-to-all-done.6, f32[]{:T(128)} %broadcast.260), dimensions={1}, to_apply=%all_to_all.59.reduce_sub_computation | reduce | bytes 2097156 | tf_op jit(solution)/shard_map/all_to_all | solution.py:190
  198.5 4.0 %reshape.404 = f32[4096,1,64]{2,1,0:T(1,128)} reshape(f32[16,16384]{1,0:T(8,128)S(1)} %reduce.9) | data formatting | bytes 2097152
  202.5 2.2 copy.97
  204.6 1.6 gather_fusion.1
  206.5 1.5 multiply_reduce_fusion
  208.0 1.3 fusion.1
  209.4 17.7 %all_to_all.78 = f32[16,16,256]{2,1,0:T(8,128)S(1)} all-to-all(f32[16,16,256]{2,1,0:T(8,128)S(1)} %bitcast.111), channel_id=1, replica_groups=mesh['ep'=16,'tp'=16] {'tp'}, dimensions={0} | all-to-all | bytes 524288 | tf_op jit(solution)/shard_map/all_to_all | solution.py:26
  227.1 14.2 %all_to_all.79 = f32[16,16,256]{2,1,0:T(8,128)S(1)} all-to-all(f32[16,16,256]{2,1,0:T(8,128)S(1)} %broadcast_in_dim.78), channel_id=1, replica_groups=mesh['ep'=16,'tp'=16] {'tp'}, dimensions={0} | all-to-all | bytes 524288 | tf_op jit(solution)/shard_map/all_to_all | solution.py:32
  241.3 0.7 fusion.17
  (81 shorter events, 6.7 us)
Async XLA Ops:
  0.6 147.9 %copy-start = (bf16[1,128,4096]{2,1,0:T(8,128)(2,1)S(1)}, bf16[1,128,4096]{2,1,0:T(8,128)(2,1)}, u32[]{:S(2)}) copy-start(bf16[1,128,4096]{2,1,0:T(8,128)(2,1)} %param.41) | copy-start | bytes 3145732
  0.6 31.9 %copy-start.8 = (s32[16]{0:T(128)S(1)}, s32[16]{0:T(128)}, u32[]{:S(2)}) copy-start(s32[16]{0:T(128)} %param.29) | copy-start | bytes 196
  2.5 13.9 %all-to-all-start.1 = ((f32[16,1,16]{2,1,0:T(1,128)}), f32[16,1,16]{2,1,0:T(1,128)S(1)}, u32[]{:S(2)}, u32[]{:S(2)}) async-start(f32[16,1,16]{2,1,0:T(1,128)} %all_to_all.53), calls=%async_computation.1 | async-start | bytes 16384 | tf_op jit(solution)/shard_map/all_to_all | solution.py:26
  16.4 12.0 %all-to-all-start = ((f32[16,16,384]{2,1,0:T(8,128)}), f32[16,16,384]{2,1,0:T(8,128)S(1)}, u32[]{:S(2)}, u32[]{:S(2)}) async-start(f32[16,16,384]{2,1,0:T(8,128)} %bitcast), calls=%async_computation | async-start | bytes 786432 | tf_op jit(solution)/shard_map/all_to_all | solution.py:26
  29.1 30.8 %copy-start.10 = (s32[256]{0:T(256)S(1)}, s32[256]{0:T(256)}, u32[]{:S(2)}) copy-start(s32[256]{0:T(256)} %param.36) | copy-start | bytes 3076
  29.1 37.3 %copy-start.5 = (bf16[128,256]{1,0:T(8,128)(2,1)S(1)}, bf16[128,256]{1,0:T(8,128)(2,1)}, u32[]{:S(2)}) copy-start(bf16[128,256]{1,0:T(8,128)(2,1)} %param.26) | copy-start | bytes 196612
  29.1 50.8 %copy-start.9 = (s32[256,2]{0,1:T(2,128)S(1)}, s32[256,2]{0,1:T(2,128)}, u32[]{:S(2)}) copy-start(s32[256,2]{0,1:T(2,128)} %param.37) | copy-start | bytes 6148
  32.5 65.7 %copy-start.11 = (bf16[256]{0:T(256)(128)(2,1)S(1)}, bf16[256]{0:T(256)(128)(2,1)}, u32[]{:S(2)}) copy-start(bf16[256]{0:T(256)(128)(2,1)} %param.32) | copy-start | bytes 1540
  32.5 65.7 %copy-start.6 = (bf16[4096]{0:T(1024)(128)(2,1)S(1)}, bf16[4096]{0:T(1024)(128)(2,1)}, u32[]{:S(2)}) copy-start(bf16[4096]{0:T(1024)(128)(2,1)} %param.31) | copy-start | bytes 24580
  32.5 74.3 %copy-start.2 = (bf16[256,256]{1,0:T(8,128)(2,1)S(1)}, bf16[256,256]{1,0:T(8,128)(2,1)}, u32[]{:S(2)}) copy-start(bf16[256,256]{1,0:T(8,128)(2,1)} %param.21) | copy-start | bytes 393220
  56.4 10.0 %all-to-all-start.2 = ((bf16[16,16,128]{2,1,0:T(8,128)(2,1)}), bf16[16,16,128]{2,1,0:T(8,128)(2,1)S(1)}, u32[]{:S(2)}, u32[]{:S(2)}) async-start(bf16[16,16,128]{2,1,0:T(8,128)(2,1)} %broadcast_in_dim.34), calls=%async_computation.2 | async-start | bytes 131072 | tf_op jit(solution)/shard_map/all_to_all | solution.py:32
  67.3 24.2 %all-to-all-start.3 = ((f32[16,16,256]{2,1,0:T(8,128)}), f32[16,16,256]{2,1,0:T(8,128)S(1)}, u32[]{:S(2)}, u32[]{:S(2)}) async-start(f32[16,16,256]{2,1,0:T(8,128)} %fusion.44), calls=%async_computation.3 | async-start | bytes 524288 | tf_op jit(solution)/shard_map/all_to_all | solution.py:26
  91.5 24.0 %copy-start.3 = (bf16[256,256]{1,0:T(8,128)(2,1)S(1)}, bf16[256,256]{1,0:T(8,128)(2,1)}, u32[]{:S(2)}) copy-start(bf16[256,256]{1,0:T(8,128)(2,1)} %param.33) | copy-start | bytes 393220
  92.2 14.6 %all-to-all-start.4 = ((f32[16,16,256]{2,1,0:T(8,128)}), f32[16,16,256]{2,1,0:T(8,128)S(1)}, u32[]{:S(2)}, u32[]{:S(2)}) async-start(f32[16,16,256]{2,1,0:T(8,128)} %broadcast_in_dim.35), calls=%async_computation.4 | async-start | bytes 524288 | tf_op jit(solution)/shard_map/all_to_all | solution.py:32
  106.9 8.9 %copy-start.4 = (bf16[256,256]{1,0:T(8,128)(2,1)S(1)}, bf16[256,256]{1,0:T(8,128)(2,1)}, u32[]{:S(2)}) copy-start(bf16[256,256]{1,0:T(8,128)(2,1)} %param.34) | copy-start | bytes 393220
  111.9 14.9 %all-to-all-start.5 = ((bf16[16,64,256]{2,1,0:T(8,128)(2,1)}), bf16[16,64,256]{2,1,0:T(8,128)(2,1)S(1)}, u32[]{:S(2)}, u32[]{:S(2)}) async-start(bf16[16,64,256]{2,1,0:T(8,128)(2,1)} %broadcast_select_fusion), calls=%async_computation.5 | async-start | bytes 1048576 | tf_op jit(solution)/shard_map/all_to_all | solution.py:175
  126.9 14.2 %all-to-all-start.7 = ((f32[16,1,8224]{2,1,0:T(1,128)}), f32[16,1,8224]{2,1,0:T(1,128)S(1)}, u32[]{:S(2)}, u32[]{:S(2)}) async-start(f32[16,1,8224]{2,1,0:T(1,128)} %all_to_all.62), calls=%async_computation.7 | async-start | bytes 1064960 | tf_op jit(solution)/shard_map/all_to_all | solution.py:26
  130.8 16.2 %copy-start.1 = (bf16[8,8,16,256]{3,1,2,0:T(8,128)(2,1)}, bf16[8,8,16,256]{3,1,2,0:T(8,128)(2,1)S(1)}, u32[]{:S(2)}) copy-start(bf16[8,8,16,256]{3,1,2,0:T(8,128)(2,1)S(1)} %copy.108) | copy-start | bytes 1572868
  142.5 31.5 %all-to-all-start.8 = ((f32[16,1,8224]{2,1,0:T(1,128)}), f32[16,1,8224]{2,1,0:T(1,128)}, u32[]{:S(2)}, u32[]{:S(2)}) async-start(f32[16,1,8224]{2,1,0:T(1,128)} %broadcast_in_dim.77), calls=%async_computation.8 | async-start | bytes 1064960 | tf_op jit(solution)/shard_map/all_to_all | solution.py:32
  151.2 29.6 %copy-start.7 = (f32[256,2]{0,1:T(2,128)S(1)}, f32[256,2]{0,1:T(2,128)}, u32[]{:S(2)}) copy-start(f32[256,2]{0,1:T(2,128)} %param.38) | copy-start | bytes 6148
  174.0 21.4 %all-to-all-start.6 = ((f32[16,1,16384]{2,1,0:T(1,128)}), f32[16,1,16384]{2,1,0:T(1,128)S(1)}, u32[]{:S(2)}, u32[]{:S(2)}) async-start(f32[16,1,16384]{2,1,0:T(1,128)} %reshape.403), calls=%async_computation.6 | async-start | bytes 2097152 | tf_op jit(solution)/shard_map/all_to_all | solution.py:190
where the time goes:
time: 243 us; the launch traced here: 242 us
  waiting for transfers between devices  64.9 us (27%)
  other arithmetic  52.5 us (22%)
  starting transfers between devices  48.6 us (20%)
  blocking collectives  31.9 us (13%)
  local copies, waits for them, and re-layouts  27.8 us (11%)
  matrix products  14.5 us (6%)
    all_to_all x4, waiting for transfers between devices, summed_on_arrival(): lax.all_to_all(tiles, axis, split_axis=0, concat_axis=0, tiled=True)  31.8 us
    all_to_all x4, starting transfers between devices, summed_on_arrival(): lax.all_to_all(tiles, axis, split_axis=0, concat_axis=0, tiled=True)  27.3 us
    another operation x3, other arithmetic  19.9 us
    unnamed x2, other arithmetic  19.5 us
    all_to_all x1, blocking collectives, summed_on_arrival(): lax.all_to_all(tiles, axis, split_axis=0, concat_axis=0, tiled=True)  17.7 us
    all_to_all x3, waiting for transfers between devices, sent_to_all(): lax.all_to_all(jnp.broadcast_to(value[None], (devices, *value.shape)), ax...  14.9 us
    all_to_all x1, blocking collectives, sent_to_all(): lax.all_to_all(jnp.broadcast_to(value[None], (devices, *value.shape)), ax...  14.2 us
    all_to_all x3, starting transfers between devices, sent_to_all(): lax.all_to_all(jnp.broadcast_to(value[None], (devices, *value.shape)), ax...  11.4 us
  transfers between devices with their start and end apart: 9, of which 8 were waited for; matrix products, arithmetic and copies ran while one was open for 17% of the time, Pallas kernels for 0%

commit v1 on v0

v1 whole, which is shorter than its diff:
```python
import functools
import math

import jax
import jax.numpy as jnp
from jax import lax
from jax.experimental import pallas as pl
from jax.experimental.pallas import tpu as pltpu
from jax.sharding import PartitionSpec as P

MESH = pl.DeviceIdType.MESH
HD = 128
EPG = 4
CAP = 4
EPS = 1e-06
F32 = jnp.float32
BF16 = jnp.bfloat16

QP, KVP, ATT, AOUT, MID, DISP, DENSE, DHID, RET, FIN, OUT = range(11)
N_PHASE = 11
VMEM_BYTES = 67_043_328


def dot(a, b):
    return jnp.dot(a, b, preferred_element_type=F32)


def dot_nt(a, b):
    return lax.dot_general(a, b, (((1,), (1,)), ((), ())), preferred_element_type=F32)


def hi_lo(col, width):
    rows = col.shape[0]
    hi = col.astype(BF16).astype(F32)
    lane = lax.broadcasted_iota(jnp.int32, (rows, width), 1)
    return jnp.where(lane < width // 2, hi, col - hi)


def un_hi_lo(pair):
    half = pair.shape[1] // 2
    return pair[:, 0:1] + pair[:, half : half + 1]


def layer(
    n_ep,
    n_tp,
    depth_all,
    tokens,
    gain,
    wq,
    wk,
    wv,
    wo,
    kc,
    vc,
    lengths,
    shift,
    gffn_row,
    wmix,
    wdg,
    wdu,
    wdd,
    rg,
    ri,
    rw,
    weg,
    weu,
    wed,
    mixed_out,
    nk_out,
    nv_out,
    tok_v,
    wq_v,
    wk_v,
    wv_v,
    wo_v,
    k_v,
    v_v,
    wdg_v,
    wdu_v,
    wdd_v,
    weg_v,
    weu_v,
    wed_v,
    onehot_v,
    combine_v,
    q_s,
    q_r,
    kv_s,
    kv_r,
    att_s,
    att_r,
    ao_s,
    ao_r,
    mid_s,
    mid_r,
    disp_s,
    disp_r,
    den_s,
    den_r,
    dh_s,
    dh_r,
    ret_s,
    ret_r,
    fin_s,
    fin_r,
    out_s,
    out_r,
    load_sem,
    send_sem,
    recv_sem,
):
    e = lax.axis_index("ep")
    t = lax.axis_index("tp")
    batch, width = tok_v.shape
    seqs = batch // n_ep
    tb = batch // n_tp
    slots = CAP * n_ep
    cache_len = k_v.shape[1]

    barrier = pltpu.get_barrier_semaphore()

    def greet(d, _):
        pl.semaphore_signal(barrier, inc=1, device_id={"ep": lax.rem(e + d, n_ep)}, device_id_type=MESH)
        return 0

    def greet_tp(d, _):
        pl.semaphore_signal(barrier, inc=1, device_id={"tp": lax.rem(t + d, n_tp)}, device_id_type=MESH)
        return 0

    lax.fori_loop(1, n_ep, greet, 0)
    lax.fori_loop(1, n_tp, greet_tp, 0)

    loads = [
        pltpu.make_async_copy(src, dst, load_sem.at[i])
        for i, (src, dst) in enumerate(
            (
                (tokens, tok_v),
                (wq, wq_v),
                (wk, wk_v),
                (wv, wv_v),
                (kc, k_v),
                (vc, v_v),
                (wo, wo_v),
                (wdg, wdg_v),
                (wdu, wdu_v),
                (weg.at[0], weg_v),
                (weu.at[0], weu_v),
                (wed.at[0], wed_v),
                (wdd, wdd_v),
            )
        )
    ]
    for load in loads:
        load.start()

    def copy_to(phase, axis, d, src, dst):
        n, me = (n_ep, e) if axis == "ep" else (n_tp, t)
        return pltpu.make_async_remote_copy(
            src_ref=src,
            dst_ref=dst,
            send_sem=send_sem.at[phase, d],
            recv_sem=recv_sem.at[phase, d],
            device_id={axis: lax.rem(me + d, n)},
            device_id_type=MESH,
        )

    def scatter(phase, axis, src, dst):
        n, me = (n_ep, e) if axis == "ep" else (n_tp, t)

        def step(d, _):
            copy_to(phase, axis, d, src.at[lax.rem(me + d, n)], dst.at[me]).start()
            return 0

        lax.fori_loop(1, n, step, 0)
        dst[me] = src[me]

    def spread(phase, axis, src, dst):
        n, me = (n_ep, e) if axis == "ep" else (n_tp, t)

        def step(d, _):
            copy_to(phase, axis, d, src, dst.at[me]).start()
            return 0

        lax.fori_loop(1, n, step, 0)
        dst[me] = src[...]

    def arrived(phase, axis, d, src, dst):
        n, me = (n_ep, e) if axis == "ep" else (n_tp, t)
        copy_to(phase, axis, d, src, dst.at[lax.rem(me - d + n, n)]).wait_recv()

    def arrive_all(phase, axis, src, dst):
        n = n_ep if axis == "ep" else n_tp

        def step(d, _):
            arrived(phase, axis, d, src, dst)
            return 0

        lax.fori_loop(1, n, step, 0)

    def sent_all(phase, axis, src, dst):
        n = n_ep if axis == "ep" else n_tp

        def step(d, _):
            copy_to(phase, axis, d, src, dst.at[0]).wait_send()
            return 0

        lax.fori_loop(1, n, step, 0)

    def total(ref, n):
        out = ref[0].astype(F32)
        for i in range(1, n):
            out = out + ref[i].astype(F32)
        return out

    loads[0].wait()
    loads[1].wait()
    tok = tok_v[...].astype(F32)
    squares = jnp.sum(tok * tok, axis=1, keepdims=True)
    scaled_in = (tok * gain[...].astype(F32)).astype(BF16)
    q_part = dot(scaled_in, wq_v[...])
    q_s[:, :, :HD] = q_part.astype(BF16).reshape(n_ep, seqs, HD)
    q_s[:, :, HD:] = hi_lo(squares, HD).astype(BF16).reshape(n_ep, seqs, HD)

    pl.semaphore_wait(barrier, n_ep + n_tp - 2)
    scatter(QP, "ep", q_s, q_r)

    loads[2].wait()
    loads[3].wait()
    kv_s[:, :, :HD] = dot(scaled_in, wk_v[...]).reshape(n_ep, seqs, HD)
    kv_s[:, :, HD:] = dot(scaled_in, wv_v[...]).reshape(n_ep, seqs, HD)
    scatter(KVP, "ep", kv_s, kv_r)

    group = rg[...].astype(F32)
    id0 = group * EPG + ri[0:1, :].astype(F32)
    id1 = group * EPG + ri[1:2, :].astype(F32)
    w0, w1 = rw[0:1, :], rw[1:2, :]
    which = lax.broadcasted_iota(jnp.int32, (n_ep, batch), 0).astype(F32)
    is0, is1 = (which == id0).astype(F32), (which == id1).astype(F32)
    before = lax.broadcasted_iota(jnp.int32, (batch, batch), 0)
    after = lax.broadcasted_iota(jnp.int32, (batch, batch), 1)
    earlier = jnp.logical_and(before < after, before // seqs == after // seqs)
    rank = dot((is0 + is1).astype(BF16), earlier.astype(F32).astype(BF16))
    block_of = (lax.broadcasted_iota(jnp.int32, (1, batch), 1) // seqs).astype(F32)
    slot0 = id0 * slots + block_of * CAP + jnp.sum(rank * is0, axis=0, keepdims=True)
    slot1 = id1 * slots + block_of * CAP + jnp.sum(rank * is1, axis=0, keepdims=True)
    slot_row = lax.broadcasted_iota(jnp.int32, (slots, batch), 0).astype(F32)
    for i in range(n_ep):
        here = slot_row + float(i * slots)
        onehot_v[i] = ((here == slot0).astype(F32) + (here == slot1).astype(F32)).astype(BF16)
    mine = slot_row + (e * slots).astype(F32)
    slot_weight = jnp.sum(
        jnp.where(mine == slot0, w0, 0.0) + jnp.where(mine == slot1, w1, 0.0), axis=1, keepdims=True
    )
    row8 = lax.broadcasted_iota(jnp.int32, (128, batch), 0)
    cols = jnp.where(row8 == 0, slot0, slot1).T
    col0, col1 = cols[:, 0:1], cols[:, 1:2]
    slot_lane = lax.broadcasted_iota(jnp.int32, (batch, width), 1).astype(F32)
    for i in range(n_ep * slots // width):
        here = slot_lane + float(i * width)
        combine_v[:, i * width : (i + 1) * width] = (
            (here == col0).astype(F32) + (here == col1).astype(F32)
        ).astype(BF16)

    arrive_all(QP, "ep", q_s.at[0], q_r)
    q_sum = total(q_r, n_ep)
    inv_first = lax.rsqrt(un_hi_lo(q_sum[:, HD:]) / depth_all + EPS)
    query = (q_sum[:, :HD] * inv_first).astype(BF16)
    loads[4].wait()
    seq_row = lax.broadcasted_iota(jnp.int32, (seqs, cache_len), 0)
    place = lax.broadcasted_iota(jnp.int32, (seqs, cache_len), 1)
    scores = jnp.zeros((seqs, cache_len), F32)
    live = jnp.zeros((seqs, cache_len), jnp.int32)
    for b in range(seqs):
        scores = jnp.where(seq_row == b, dot_nt(query, k_v[b]), scores)
        live = jnp.where(seq_row == b, lengths[b], live)
    is_live = place < live
    scores = scores / math.sqrt(HD) + shift[0]
    tail = jnp.log1p(jnp.exp(-jnp.abs(scores)))
    soft = jnp.where(is_live, jnp.maximum(scores, 0.0) + tail, 0.0)
    running = soft
    step = 1
    while step < cache_len:
        moved = pltpu.roll(running, cache_len - step, 1)
        running = running + jnp.where(place < cache_len - step, moved, 0.0)
        step *= 2
    later = running - soft
    stick = jnp.where(is_live, jnp.exp(jnp.minimum(scores, 0.0) - tail - later), 0.0).astype(BF16)
    loads[5].wait()
    out_row = lax.broadcasted_iota(jnp.int32, (seqs, HD), 0)
    attended = jnp.zeros((seqs, HD), F32)
    for b in range(seqs):
        attended = jnp.where(out_row == b, dot(stick, v_v[b]), attended)
    att_s[...] = attended.astype(BF16)
    spread(ATT, "ep", att_s, att_r)

    arrive_all(KVP, "ep", kv_s.at[0], kv_r)
    kv_sum = total(kv_r, n_ep) * inv_first
    nk_out[...] = kv_sum[:, :HD].astype(BF16)
    nv_out[...] = kv_sum[:, HD:].astype(BF16)

    loads[6].wait()
    arrive_all(ATT, "ep", att_s, att_r)
    ao_s[...] = dot(att_r[...].reshape(batch, HD), wo_v[...]).astype(BF16).reshape(n_tp, tb, width)
    scatter(AOUT, "tp", ao_s, ao_r)
    arrive_all(AOUT, "tp", ao_s.at[0], ao_r)
    own_rows = pl.ds(pl.multiple_of(t * tb, tb), tb)
    middle_own = (tok_v[own_rows, :].astype(F32) + total(ao_r, n_tp)).astype(BF16)
    mid_s[...] = middle_own
    spread(MID, "tp", mid_s, mid_r)
    arrive_all(MID, "tp", mid_s, mid_r)
    middle = mid_r[...].reshape(batch, width)

    def dispatch(d, _):
        to = lax.rem(e + d, n_ep)
        disp_s[to] = dot(onehot_v[to], middle).astype(BF16)
        copy_to(DISP, "ep", d, disp_s.at[to], disp_r.at[e]).start()
        return 0

    lax.fori_loop(1, n_ep, dispatch, 0)
    disp_r[e] = dot(onehot_v[e], middle).astype(BF16)

    mid_f = middle.astype(F32)
    mid_squares = jnp.sum(mid_f * mid_f, axis=1, keepdims=True)
    my_gain = gffn_row[:, pl.ds(pl.multiple_of(e * width, width), width)].astype(F32)
    scaled_mid = (mid_f * my_gain).astype(BF16)
    mix = jnp.sum(scaled_mid.astype(F32) * wmix[...].astype(F32), axis=1, keepdims=True)
    hidden_cols = wdg_v.shape[1]
    loads[7].wait()
    loads[8].wait()
    den_s[:, :, :hidden_cols] = dot(scaled_mid, wdg_v[...]).astype(BF16).reshape(n_ep, seqs, hidden_cols)
    den_s[:, :, hidden_cols : 2 * hidden_cols] = (
        dot(scaled_mid, wdu_v[...]).astype(BF16).reshape(n_ep, seqs, hidden_cols)
    )
    lane = lax.broadcasted_iota(jnp.int32, (batch, 128), 1)
    pair = jnp.where(lane % 2 == 0, hi_lo(mix, 128), hi_lo(mid_squares, 128))
    den_s[:, :, 2 * hidden_cols :] = pair.astype(BF16).reshape(n_ep, seqs, 128)
    scatter(DENSE, "ep", den_s, den_r)

    loads[9].wait()
    loads[10].wait()

    def expert_part(src, carry):
        gate, up, sq = carry
        rows_f = disp_r[src].astype(F32)
        at = pl.ds(pl.multiple_of(src * width, width), width)
        scaled = (rows_f * gffn_row[:, at].astype(F32)).astype(BF16)
        gate = gate + dot(scaled, weg_v[at, :])
        up = up + dot(scaled, weu_v[at, :])
        s2 = rows_f * rows_f
        for i in range(width // 128):
            sq = sq + s2[:, i * 128 : (i + 1) * 128]
        return gate, up, sq

    def expert_step(d, carry):
        arrived(DISP, "ep", d, disp_s.at[0], disp_r)
        return expert_part(lax.rem(e - d + n_ep, n_ep), carry)

    ff = weg_v.shape[1]
    zero = jnp.zeros((slots, ff), F32)
    carry = expert_part(e, (zero, zero, jnp.zeros((slots, 128), F32)))
    gate, up, sq = lax.fori_loop(1, n_ep, expert_step, carry)
    inv_rows = lax.rsqrt(jnp.sum(sq, axis=1, keepdims=True) / depth_all + EPS)
    gate = gate * inv_rows
    hidden = (gate / (1.0 + jnp.exp(-gate)) * (up * inv_rows)).astype(BF16)
    loads[11].wait()

    def give_back(d, _):
        to = lax.rem(e + d, n_ep)
        at = pl.ds(pl.multiple_of(to * width, width), width)
        ret_s[to] = (dot(hidden, wed_v[:, at]) * slot_weight).astype(BF16)
        copy_to(RET, "ep", d, ret_s.at[to], ret_r.at[e]).start()
        return 0

    lax.fori_loop(1, n_ep, give_back, 0)
    own_at = pl.ds(pl.multiple_of(e * width, width), width)
    ret_r[e] = (dot(hidden, wed_v[:, own_at]) * slot_weight).astype(BF16)

    arrive_all(DENSE, "ep", den_s.at[0], den_r)
    dense = total(den_r, n_ep)
    extra = dense[:, 2 * hidden_cols :]
    mix_sum = extra[:, 0:1] + extra[:, 64:65]
    sq_sum = extra[:, 1:2] + extra[:, 65:66]
    inv_second = lax.rsqrt(sq_sum / depth_all + EPS)
    pre = dense[:, :hidden_cols] * inv_second
    lin = dense[:, hidden_cols : 2 * hidden_cols] * inv_second
    dh_s[:, :hidden_cols] = (pre / (1.0 + jnp.exp(-pre)) * lin).astype(BF16)
    mix_gate = 1.0 / (1.0 + jnp.exp(-mix_sum * inv_second))
    dh_s[:, hidden_cols:] = hi_lo(mix_gate, 128).astype(BF16)
    spread(DHID, "ep", dh_s, dh_r)
    loads[12].wait()
    arrive_all(DHID, "ep", dh_s, dh_r)
    dh_all = dh_r[...].reshape(batch, hidden_cols + 128)
    gate_all = un_hi_lo(dh_all[:, hidden_cols:].astype(F32))
    part = dot(dh_all[:, :hidden_cols], wdd_v[...]) * gate_all

    arrive_all(RET, "ep", ret_s.at[0], ret_r)
    part = part + dot(combine_v[...], ret_r[...].reshape(n_ep * slots, width))
    fin_s[...] = part.astype(BF16).reshape(n_tp, tb, width)
    scatter(FIN, "tp", fin_s, fin_r)
    arrive_all(FIN, "tp", fin_s.at[0], fin_r)
    out_s[...] = (mid_s[...].astype(F32) + total(fin_r, n_tp)).astype(BF16)
    spread(OUT, "tp", out_s, out_r)
    arrive_all(OUT, "tp", out_s, out_r)
    mixed_out[...] = out_r[...].reshape(batch, width)

    sent_all(QP, "ep", q_s.at[0], q_r)
    sent_all(KVP, "ep", kv_s.at[0], kv_r)
    sent_all(ATT, "ep", att_s, att_r)
    sent_all(AOUT, "tp", ao_s.at[0], ao_r)
    sent_all(MID, "tp", mid_s, mid_r)
    sent_all(DISP, "ep", disp_s.at[0], disp_r)
    sent_all(DENSE, "ep", den_s.at[0], den_r)
    sent_all(DHID, "ep", dh_s, dh_r)
    sent_all(RET, "ep", ret_s.at[0], ret_r)
    sent_all(FIN, "tp", fin_s.at[0], fin_r)
    sent_all(OUT, "tp", out_s, out_r)


def on_device(n_ep, n_tp, *args):
    (
        tokens,
        gain_attn,
        w_query,
        w_key,
        w_value,
        w_output,
        key_cache,
        value_cache,
        lengths,
        score_shift,
        gain_ffn,
        w_mix,
        w_dense_gate,
        w_dense_up,
        w_dense_down,
        route_group,
        route_inner,
        route_weight,
        w_exp_gate,
        w_exp_up,
        w_exp_down,
    ) = args
    batch, width = tokens.shape
    seqs, tb = batch // n_ep, batch // n_tp
    slots = CAP * n_ep
    dense_cols = w_dense_gate.shape[1]
    n = max(n_ep, n_tp)
    anywhere = pl.BlockSpec(memory_space=pl.ANY)
    vmem = pl.BlockSpec(memory_space=pltpu.VMEM)
    smem = pl.BlockSpec(memory_space=pltpu.SMEM)

    def like(a, skip=0):
        return pltpu.VMEM(a.shape[skip:], a.dtype)

    def both(*shape, dtype=BF16):
        return [pltpu.VMEM(shape, dtype)] * 2

    return pl.pallas_call(
        functools.partial(layer, n_ep, n_tp, width * n_ep),
        out_shape=(
            jax.ShapeDtypeStruct((batch, width), BF16),
            jax.ShapeDtypeStruct((seqs, HD), BF16),
            jax.ShapeDtypeStruct((seqs, HD), BF16),
        ),
        in_specs=[
            anywhere, vmem, anywhere, anywhere, anywhere, anywhere, anywhere, anywhere,
            smem, smem, vmem, vmem, anywhere, anywhere, anywhere, vmem, vmem, vmem,
            anywhere, anywhere, anywhere,
        ],
        out_specs=(vmem, vmem, vmem),
        scratch_shapes=[
            like(tokens), like(w_query), like(w_key), like(w_value), like(w_output),
            like(key_cache), like(value_cache),
            like(w_dense_gate), like(w_dense_up), like(w_dense_down),
            like(w_exp_gate, 1), like(w_exp_up, 1), like(w_exp_down, 1),
            pltpu.VMEM((n_ep, slots, batch), BF16),
            pltpu.VMEM((batch, n_ep * slots), BF16),
            *both(n_ep, seqs, 2 * HD),
            *both(n_ep, seqs, 2 * HD, dtype=F32),
            pltpu.VMEM((seqs, HD), BF16), pltpu.VMEM((n_ep, seqs, HD), BF16),
            *both(n_tp, tb, width),
            pltpu.VMEM((tb, width), BF16), pltpu.VMEM((n_tp, tb, width), BF16),
            *both(n_ep, slots, width),
            *both(n_ep, seqs, 2 * dense_cols + 128),
            pltpu.VMEM((seqs, dense_cols + 128), BF16),
            pltpu.VMEM((n_ep, seqs, dense_cols + 128), BF16),
            *both(n_ep, slots, width),
            *both(n_tp, tb, width),
            pltpu.VMEM((tb, width), BF16), pltpu.VMEM((n_tp, tb, width), BF16),
            pltpu.SemaphoreType.DMA((13,)),
            pltpu.SemaphoreType.DMA((N_PHASE, n)),
            pltpu.SemaphoreType.DMA((N_PHASE, n)),
        ],
        compiler_params=pltpu.CompilerParams(
            collective_id=0, has_side_effects=True, vmem_limit_bytes=VMEM_BYTES
        ),
        name="decode_layer",
    )(
        tokens, gain_attn[None, :], w_query, w_key, w_value, w_output, key_cache, value_cache,
        lengths, score_shift, gain_ffn[None, :], w_mix[None, :],
        w_dense_gate, w_dense_up, w_dense_down,
        route_group[None, :], route_inner.T, route_weight.T,
        w_exp_gate, w_exp_up, w_exp_down,
    )


def solution(mesh):
    placed = (
        P(None, "ep"),
        P("ep"),
        P("ep", "tp"),
        P("ep", "tp"),
        P("ep", "tp"),
        P("tp", "ep"),
        P("ep", None, "tp"),
        P("ep", None, "tp"),
        P("ep"),
        P("tp"),
        P(),
        P("ep"),
        P("ep", "tp"),
        P("ep", "tp"),
        P("tp", "ep"),
        P(),
        P(),
        P(),
        P("ep", None, "tp"),
        P("ep", None, "tp"),
        P("ep", "tp", None),
    )
    return jax.shard_map(
        functools.partial(on_device, mesh.shape["ep"], mesh.shape["tp"]),
        mesh=mesh,
        in_specs=placed,
        out_specs=(P(None, "ep"), P("ep", "tp"), P("ep", "tp")),
        check_vma=False,
    )
```

time: 243 us -> 84.1 us (0.35)
  Pallas kernels: 0 us -> 74.7 us
  waiting for transfers between devices: 64.9 us -> 0 us
  other arithmetic: 52.5 us -> 0 us
  starting transfers between devices: 48.6 us -> 0 us
  blocking collectives: 31.9 us -> 0 us
  local copies, waits for them, and re-layouts: 27.8 us -> 7.86 us
  matrix products: 14.5 us -> 0 us
    pallas_call x0 -> x1, Pallas kernels: none -> 74.7 us  [on_device(): pl.pallas_call(functools.partial(layer, n_ep, n_tp, width * n_ep), out_sh...]
    all_to_all x9 -> x0, waiting for transfers between devices: 64.9 us -> none  [the longest x4 31.8 us: summed_on_arrival(): lax.all_to_all(tiles, axis, split_axis=0, concat_axis=0, tiled=True)]
    all_to_all x9 -> x0, starting transfers between devices: 48.6 us -> none  [the longest x4 27.3 us: summed_on_arrival(): lax.all_to_all(tiles, axis, split_axis=0, concat_axis=0, tiled=True)]
    all_to_all x2 -> x0, blocking collectives: 31.9 us -> none  [the longest x1 17.7 us: summed_on_arrival(): lax.all_to_all(tiles, axis, split_axis=0, concat_axis=0, tiled=True)]
    another operation x4 -> x0, other arithmetic: 20.8 us -> none
    unnamed x2 -> x0, other arithmetic: 19.5 us -> none
    dot_general x10 -> x0, matrix products: 14.5 us -> none  [the longest x1 3.39 us: on_device(): jnp.einsum('bhd,blhd->bhl', head_query, head_keys, preferred_element_type...]
    gather x3 -> x0, local copies, waits for them, and re-layouts: 5.82 us -> none  [the longest x1 3.94 us: on_device(): jnp.take(padded_middle, slot_table, axis=0)]
  transfers between devices with their start and end apart: 9 -> 0, of which waited for: 8 -> 0; matrix products, arithmetic and copies ran while one was open for 17% -> 0% of each run, Pallas kernels for 0% -> 0%
where the time goes in v1:
time: 84.1 us; the launch traced here: 83.9 us
  Pallas kernels  74.7 us (89%)
  local copies, waits for them, and re-layouts  7.86 us (9%)
  between operations  1.29 us (2%)
    pallas_call x1, Pallas kernels, on_device(): pl.pallas_call(functools.partial(layer, n_ep, n_tp, width * n_ep), out_sh...  74.7 us
    unnamed x3, local copies, waits for them, and re-layouts  4.11 us

profile of v1, /device:TPU:1, one launch (start us, length us, event | category | flops | bytes accessed | tf_op | source)
XLA Modules:
  0.0 83.9 jit_solution(3198257833391171694)
XLA Ops:
  1.3 1.2 %broadcast_in_dim.12.gain = bf16[1,256]{1,0:T(2,128)(2,1)} reshape(bf16[256]{0:T(256)(128)(2,1)} %param.22) | data formatting | bytes 1024 | tf_op jit(solution)/shard_map/broadcast_in_dim | solution.py:500
  2.5 1.2 %broadcast_in_dim.14.wmix = bf16[1,256]{1,0:T(2,128)(2,1)} reshape(bf16[256]{0:T(256)(128)(2,1)} %param.32) | data formatting | bytes 1024 | tf_op jit(solution)/shard_map/broadcast_in_dim | solution.py:501
  3.7 1.3 %broadcast_in_dim.13.gffn_row = bf16[1,4096]{1,0:T(2,128)(2,1)} reshape(bf16[4096]{0:T(1024)(128)(2,1)} %param.31) | data formatting | bytes 16384 | tf_op jit(solution)/shard_map/broadcast_in_dim | solution.py:501
  5.0 74.7 %decode_layer.1 = (bf16[256,256]{1,0:T(8,128)(2,1)}, bf16[16,128]{1,0:T(8,128)(2,1)}, bf16[16,128]{1,0:T(8,128)(2,1)}) custom-call(bf16[256,256]{1,0:T(8,128)(2,1)} %tokens.1, bf16[1,256]{1,0:T(2,128)(2,1)} %broadcast_in_dim.12.gain, bf16[256,128]{1,0:T(8,128)(2,1)} %wq.1, bf16[256,128]{1,0:T(8,128)(2,1)} %wk.1, bf16[256,128]{1,0:T(8,128)(2,1)} %wv.1, ...), custom_call_target="tpu_custom_call" | custom-call | tf_op jit(solution)/shard_map/decode_layer/pallas_call | solution.py:459
  79.7 1.6 %copy.28 = bf16[256,256]{1,0:T(8,128)(2,1)} copy(bf16[256,256]{1,0:T(8,128)(2,1)} %get-tuple-element.6) | data formatting | bytes 262144
  81.3 1.3 %copy.29 = bf16[16,128]{1,0:T(8,128)(2,1)} copy(bf16[16,128]{1,0:T(8,128)(2,1)} %get-tuple-element.7) | data formatting | bytes 8192
  82.6 1.3 %copy.30 = bf16[16,128]{1,0:T(8,128)(2,1)} copy(bf16[16,128]{1,0:T(8,128)(2,1)} %get-tuple-element.8) | data formatting | bytes 8192

commit v2 on v1

v2 whole, which is shorter than its diff:
```python
import functools
import math

import jax
import jax.numpy as jnp
from jax import lax
from jax.experimental import pallas as pl
from jax.experimental.pallas import tpu as pltpu
from jax.sharding import PartitionSpec as P

MESH = pl.DeviceIdType.MESH
HD = 128
EPG = 4
CAP = 4
EPS = 1e-06
F32 = jnp.float32
BF16 = jnp.bfloat16

QP, KVP, ATT, AOUT, MID, DISP, DENSE, DHID, RET, FIN, OUT = range(11)
N_PHASE = 11
WDOWN, HID, DPART, N_PAIR = 15, 16, 17, 18
VMEM_BYTES = 67_043_328 - 0 * 1024


def dot(a, b):
    return jnp.dot(a, b, preferred_element_type=F32)


def dot_nt(a, b):
    return lax.dot_general(a, b, (((1,), (1,)), ((), ())), preferred_element_type=F32)


def hi_lo(col, width):
    rows = col.shape[0]
    hi = col.astype(BF16).astype(F32)
    lane = lax.broadcasted_iota(jnp.int32, (rows, width), 1)
    return jnp.where(lane < width // 2, hi, col - hi)


def un_hi_lo(pair):
    half = pair.shape[1] // 2
    return pair[:, 0:1] + pair[:, half : half + 1]


def ring(d, n):
    return min(d % n, n - d % n)


def offsets_ep(n):
    if n != 16:
        return [(0, d) for d in range(1, n)], n
    pairs = [(a, b) for a in range(4) for b in range(4) if a or b]
    return sorted(pairs, key=lambda p: -ring(p[0], 4) - ring(p[1], 4)), 4


def offsets_tp(n):
    pairs = [(a, b) for a in range(n // 2) for b in range(2) if a or b]
    return sorted(pairs, key=lambda p: -ring(p[0], n // 2) * 2 - p[1]), 2


def partners(me, offsets, minor, n):
    major = n // minor
    hi, lo = me // minor, lax.rem(me, minor)
    to = [lax.rem(hi + a, major) * minor + lax.rem(lo + b, minor) for a, b in offsets]
    back = [lax.rem(hi - a + major, major) * minor + lax.rem(lo - b + minor, minor) for a, b in offsets]
    return to, back


def layer(
    n_ep,
    n_tp,
    depth_all,
    tokens,
    gain,
    wq,
    wk,
    wv,
    wo,
    kc,
    vc,
    lengths,
    shift,
    gffn,
    wmix,
    wdg,
    wdu,
    wdd,
    rg,
    ri,
    rw,
    weg,
    weu,
    wed,
    mixed_out,
    nk_out,
    nv_out,
    tok_v,
    wq_v,
    wk_v,
    wv_v,
    wo_v,
    k_v,
    v_v,
    wdg_v,
    wdu_v,
    wdd_v,
    wgu_v,
    wed_v,
    wed_o,
    gain_v,
    len_v,
    shift_v,
    gffn_v,
    wmix_v,
    rg_v,
    ri_v,
    rw_v,
    gffn_row,
    onehot_v,
    combine_v,
    q_s,
    q_r,
    kv_s,
    kv_r,
    att_s,
    att_r,
    ao_s,
    ao_r,
    mid_s,
    mid_r,
    disp_s,
    disp_r,
    disp_o,
    den_s,
    den_r,
    dh_s,
    dh_r,
    hid_s,
    hid_r,
    ret_s,
    ret_r,
    dp_s,
    dp_r,
    fin_s,
    fin_r,
    out_s,
    out_r,
    load_sem,
    send_sem,
    recv_sem,
    pair_send,
    pair_recv,
):
    e = lax.axis_index("ep")
    t = lax.axis_index("tp")
    batch, width = tok_v.shape
    seqs = batch // n_ep
    tb = batch // n_tp
    slots = CAP * n_ep
    cache_len = k_v.shape[1]
    ff = wgu_v.shape[1] // 2

    ep_to, ep_from = partners(e, *offsets_ep(n_ep), n_ep)
    tp_to, tp_from = partners(t, *offsets_tp(n_tp), n_tp)
    z, core = t // 2, lax.rem(t, 2)
    n_z = n_tp // 2
    far_z = sorted(range(1, n_z), key=lambda a: -ring(a, n_z))
    z_to = [lax.rem(z + a, n_z) for a in far_z]
    z_from = [lax.rem(z - a + n_z, n_z) for a in far_z]
    to_of = {"ep": ep_to, "tp": tp_to, "z": z_to}
    from_of = {"ep": ep_from, "tp": tp_from, "z": z_from}
    me_of = {"ep": e, "tp": t, "z": z}
    half = width // 2
    own_half = pl.ds(pl.multiple_of(core * half, half), half)
    other_half = pl.ds(pl.multiple_of((1 - core) * half, half), half)

    barrier = pltpu.get_barrier_semaphore()
    for axis in ("ep", "tp"):
        for peer in to_of[axis]:
            pl.semaphore_signal(barrier, inc=1, device_id={axis: peer}, device_id_type=MESH)

    loads = [
        pltpu.make_async_copy(src, dst, load_sem.at[i])
        for i, (src, dst) in enumerate(
            (
                (tokens, tok_v),
                (wq, wq_v),
                (wk, wk_v),
                (wv, wv_v),
                (kc, k_v),
                (vc, v_v),
                (wo, wo_v),
                (wdg, wdg_v),
                (wdu, wdu_v),
                (weg.at[0], wgu_v.at[:, :ff]),
                (weu.at[0], wgu_v.at[:, ff:]),
                (wed.at[0], wed_v),
                (wdd, wdd_v),
                (gain, gain_v),
                (lengths, len_v),
                (shift, shift_v),
                (gffn, gffn_v),
                (wmix, wmix_v),
                (rg, rg_v),
                (ri, ri_v),
                (rw, rw_v),
            )
        )
    ]
    for load in loads:
        load.start()

    def copy_to(phase, axis, k, src, dst):
        return pltpu.make_async_remote_copy(
            src_ref=src,
            dst_ref=dst,
            send_sem=send_sem.at[phase, k],
            recv_sem=recv_sem.at[phase, k],
            device_id={"tp": to_of[axis][k] * 2 + core} if axis == "z" else {axis: to_of[axis][k]},
            device_id_type=MESH,
        )

    def to_partner(k, src, dst):
        return pltpu.make_async_remote_copy(
            src_ref=src,
            dst_ref=dst,
            send_sem=pair_send.at[k],
            recv_sem=pair_recv.at[k],
            device_id={"tp": 2 * z + 1 - core},
            device_id_type=MESH,
        )

    def scatter(phase, axis, src, dst):
        me = me_of[axis]
        for k, to in enumerate(to_of[axis]):
            copy_to(phase, axis, k, src.at[to], dst.at[me]).start()
        dst[me] = src[me]

    def spread(phase, axis, src, dst):
        me = me_of[axis]
        for k in range(len(to_of[axis])):
            copy_to(phase, axis, k, src, dst.at[me]).start()
        dst[me] = src[...]

    def arrived(phase, axis, k, src, dst):
        copy_to(phase, axis, k, src, dst.at[from_of[axis][k]]).wait_recv()

    def arrive_all(phase, axis, src, dst):
        for k in range(len(to_of[axis])):
            arrived(phase, axis, k, src, dst)

    def sent_all(phase, axis, src, dst):
        for k in range(len(to_of[axis])):
            copy_to(phase, axis, k, src, dst.at[0]).wait_send()

    def total(ref, n):
        out = ref[0].astype(F32)
        for i in range(1, n):
            out = out + ref[i].astype(F32)
        return out

    loads[0].wait()
    loads[1].wait()
    loads[13].wait()
    tok = tok_v[...].astype(F32)
    squares = jnp.sum(tok * tok, axis=1, keepdims=True)
    scaled_in = (tok * gain_v[...].astype(F32)[None, :]).astype(BF16)
    q_part = dot(scaled_in, wq_v[...])
    q_s[:, :, :HD] = q_part.astype(BF16).reshape(n_ep, seqs, HD)
    q_s[:, :, HD:] = hi_lo(squares, HD).astype(BF16).reshape(n_ep, seqs, HD)

    pl.semaphore_wait(barrier, n_ep + n_tp - 2)
    scatter(QP, "ep", q_s, q_r)

    loads[2].wait()
    loads[3].wait()
    kv_s[:, :, :HD] = dot(scaled_in, wk_v[...]).reshape(n_ep, seqs, HD)
    kv_s[:, :, HD:] = dot(scaled_in, wv_v[...]).reshape(n_ep, seqs, HD)

    for i in range(14, 21):
        loads[i].wait()
    gffn_row[...] = gffn_v[...].astype(F32)[None, :]
    group = rg_v[...].astype(F32)[None, :]
    id0 = group * EPG + ri_v[0:1, :].astype(F32)
    id1 = group * EPG + ri_v[1:2, :].astype(F32)
    w0, w1 = rw_v[0:1, :], rw_v[1:2, :]
    which = lax.broadcasted_iota(jnp.int32, (n_ep, batch), 0).astype(F32)
    is0, is1 = (which == id0).astype(F32), (which == id1).astype(F32)
    before = lax.broadcasted_iota(jnp.int32, (batch, batch), 0)
    after = lax.broadcasted_iota(jnp.int32, (batch, batch), 1)
    earlier = jnp.logical_and(before < after, before // seqs == after // seqs)
    rank = dot((is0 + is1).astype(BF16), earlier.astype(F32).astype(BF16))
    block_of = (lax.broadcasted_iota(jnp.int32, (1, batch), 1) // seqs).astype(F32)
    slot0 = id0 * slots + block_of * CAP + jnp.sum(rank * is0, axis=0, keepdims=True)
    slot1 = id1 * slots + block_of * CAP + jnp.sum(rank * is1, axis=0, keepdims=True)
    slot_row = lax.broadcasted_iota(jnp.int32, (slots, batch), 0).astype(F32)
    for i in range(n_ep):
        here = slot_row + float(i * slots)
        onehot_v[i] = ((here == slot0).astype(F32) + (here == slot1).astype(F32)).astype(BF16)
    mine = slot_row + (e * slots).astype(F32)
    slot_weight = jnp.sum(
        jnp.where(mine == slot0, w0, 0.0) + jnp.where(mine == slot1, w1, 0.0), axis=1, keepdims=True
    )
    row8 = lax.broadcasted_iota(jnp.int32, (128, batch), 0)
    cols = jnp.where(row8 == 0, slot0, slot1).T
    col0, col1 = cols[:, 0:1], cols[:, 1:2]
    slot_lane = lax.broadcasted_iota(jnp.int32, (batch, width), 1).astype(F32)
    for i in range(n_ep * slots // width):
        here = slot_lane + float(i * width)
        combine_v[:, i * width : (i + 1) * width] = (
            (here == col0).astype(F32) + (here == col1).astype(F32)
        ).astype(BF16)

    loads[11].wait()
    for i in range(n_ep):
        at = pl.ds(pl.multiple_of(i * width + (1 - core) * half, half), half)
        to_partner(WDOWN, wed_v.at[:, at], wed_o.at[:, i * half : (i + 1) * half]).start()

    arrive_all(QP, "ep", q_s.at[0], q_r)
    q_sum = total(q_r, n_ep)
    inv_first = lax.rsqrt(un_hi_lo(q_sum[:, HD:]) / depth_all + EPS)
    query = (q_sum[:, :HD] * inv_first).astype(BF16)
    loads[4].wait()
    seq_row = lax.broadcasted_iota(jnp.int32, (seqs, cache_len), 0)
    place = lax.broadcasted_iota(jnp.int32, (seqs, cache_len), 1)
    scores = jnp.zeros((seqs, cache_len), F32)
    live = jnp.zeros((seqs, cache_len), jnp.int32)
    for b in range(seqs):
        scores = jnp.where(seq_row == b, dot_nt(query, k_v[b]), scores)
        live = jnp.where(seq_row == b, len_v[b], live)
    is_live = place < live
    scores = scores / math.sqrt(HD) + shift_v[0]
    tail = jnp.log1p(jnp.exp(-jnp.abs(scores)))
    soft = jnp.where(is_live, jnp.maximum(scores, 0.0) + tail, 0.0)
    running = soft
    step = 1
    while step < cache_len:
        moved = pltpu.roll(running, cache_len - step, 1)
        running = running + jnp.where(place < cache_len - step, moved, 0.0)
        step *= 2
    later = running - soft
    stick = jnp.where(is_live, jnp.exp(jnp.minimum(scores, 0.0) - tail - later), 0.0).astype(BF16)
    loads[5].wait()
    out_row = lax.broadcasted_iota(jnp.int32, (seqs, HD), 0)
    attended = jnp.zeros((seqs, HD), F32)
    for b in range(seqs):
        attended = jnp.where(out_row == b, dot(stick, v_v[b]), attended)
    att_s[...] = attended.astype(BF16)
    spread(ATT, "ep", att_s, att_r)

    loads[6].wait()
    arrive_all(ATT, "ep", att_s, att_r)
    ao_s[...] = dot(att_r[...].reshape(batch, HD), wo_v[...]).astype(BF16).reshape(n_tp, tb, width)
    scatter(AOUT, "tp", ao_s, ao_r)
    scatter(KVP, "ep", kv_s, kv_r)
    arrive_all(AOUT, "tp", ao_s.at[0], ao_r)
    own_rows = pl.ds(pl.multiple_of(t * tb, tb), tb)
    middle_own = (tok_v[own_rows, :].astype(F32) + total(ao_r, n_tp)).astype(BF16)
    mid_s[...] = middle_own
    spread(MID, "tp", mid_s, mid_r)

    arrive_all(KVP, "ep", kv_s.at[0], kv_r)
    kv_sum = total(kv_r, n_ep) * inv_first
    nk_out[...] = kv_sum[:, :HD].astype(BF16)
    nv_out[...] = kv_sum[:, HD:].astype(BF16)

    arrive_all(MID, "tp", mid_s, mid_r)
    middle = mid_r[...].reshape(batch, width)

    mid_own = mid_r[:, :, own_half].reshape(batch, half)
    mid_other = mid_r[:, :, other_half].reshape(batch, half)
    for k, to in enumerate(ep_to):
        disp_s[to] = dot(onehot_v[to], mid_own).astype(BF16)
        copy_to(DISP, "ep", k, disp_s.at[to], disp_r.at[e]).start()
    disp_r[e] = dot(onehot_v[e], mid_own).astype(BF16)
    disp_o[e] = dot(onehot_v[e], mid_other).astype(BF16)

    mid_f = middle.astype(F32)
    mid_squares = jnp.sum(mid_f * mid_f, axis=1, keepdims=True)
    my_gain = gffn_row[:, pl.ds(pl.multiple_of(e * width, width), width)]
    scaled_mid = (mid_f * my_gain).astype(BF16)
    mix = jnp.sum(scaled_mid.astype(F32) * wmix_v[...].astype(F32)[None, :], axis=1, keepdims=True)
    hidden_cols = wdg_v.shape[1]
    loads[7].wait()
    loads[8].wait()
    den_s[:, :, :hidden_cols] = dot(scaled_mid, wdg_v[...]).astype(BF16).reshape(n_ep, seqs, hidden_cols)
    den_s[:, :, hidden_cols : 2 * hidden_cols] = (
        dot(scaled_mid, wdu_v[...]).astype(BF16).reshape(n_ep, seqs, hidden_cols)
    )
    lane = lax.broadcasted_iota(jnp.int32, (batch, 128), 1)
    pair = jnp.where(lane % 2 == 0, hi_lo(mix, 128), hi_lo(mid_squares, 128))
    den_s[:, :, 2 * hidden_cols :] = pair.astype(BF16).reshape(n_ep, seqs, 128)
    scatter(DENSE, "ep", den_s, den_r)

    loads[9].wait()
    loads[10].wait()

    def expert_part(ref, src, part, carry):
        acc, sq = carry
        rows_f = ref[src].astype(F32)
        at = pl.ds(pl.multiple_of(src * width + part * half, half), half)
        scaled = (rows_f * gffn_row[:, at]).astype(BF16)
        return acc + dot(scaled, wgu_v[at, :]), sq + rows_f * rows_f

    carry = (jnp.zeros((slots, 2 * ff), F32), jnp.zeros((slots, half), F32))
    carry = expert_part(disp_r, e, core, carry)
    carry = expert_part(disp_o, e, 1 - core, carry)
    nearest_first = list(reversed(range(n_ep - 1)))
    for k in nearest_first:
        arrived(DISP, "ep", k, disp_s.at[0], disp_r)
        to_partner(k, disp_r.at[ep_from[k]], disp_o.at[ep_from[k]]).start()
        carry = expert_part(disp_r, ep_from[k], core, carry)
    for k in nearest_first:
        to_partner(k, disp_r.at[ep_from[k]], disp_o.at[ep_from[k]]).wait_recv()
        carry = expert_part(disp_o, ep_from[k], 1 - core, carry)
    acc, sq = carry
    inv_rows = lax.rsqrt(jnp.sum(sq, axis=1, keepdims=True) / depth_all + EPS)
    gate = acc[:, :ff] * inv_rows
    hid_s[...] = (gate / (1.0 + jnp.exp(-gate)) * (acc[:, ff:] * inv_rows)).astype(BF16)
    to_partner(HID, hid_s, hid_r).start()
    to_partner(WDOWN, wed_o, wed_o).wait_recv()
    to_partner(HID, hid_s, hid_r).wait_recv()
    hidden, hidden_o = hid_s[...], hid_r[...]

    def down(to):
        at = pl.ds(pl.multiple_of(to * width + core * half, half), half)
        at_o = pl.ds(pl.multiple_of(to * half, half), half)
        return ((dot(hidden, wed_v[:, at]) + dot(hidden_o, wed_o[:, at_o])) * slot_weight).astype(BF16)

    for k, to in enumerate(ep_to):
        ret_s[to] = down(to)
        copy_to(RET, "ep", k, ret_s.at[to], ret_r.at[e]).start()
    ret_r[e] = down(e)

    arrive_all(DENSE, "ep", den_s.at[0], den_r)
    dense = total(den_r, n_ep)
    extra = dense[:, 2 * hidden_cols :]
    mix_sum = extra[:, 0:1] + extra[:, 64:65]
    sq_sum = extra[:, 1:2] + extra[:, 65:66]
    inv_second = lax.rsqrt(sq_sum / depth_all + EPS)
    pre = dense[:, :hidden_cols] * inv_second
    lin = dense[:, hidden_cols : 2 * hidden_cols] * inv_second
    dh_s[:, :hidden_cols] = (pre / (1.0 + jnp.exp(-pre)) * lin).astype(BF16)
    mix_gate = 1.0 / (1.0 + jnp.exp(-mix_sum * inv_second))
    dh_s[:, hidden_cols:] = hi_lo(mix_gate, 128).astype(BF16)
    spread(DHID, "ep", dh_s, dh_r)
    loads[12].wait()
    arrive_all(DHID, "ep", dh_s, dh_r)
    dh_all = dh_r[...].reshape(batch, hidden_cols + 128)
    gate_all = un_hi_lo(dh_all[:, hidden_cols:].astype(F32))
    dense_in = dh_all[:, :hidden_cols]
    dp_s[...] = dot(dense_in, wdd_v[:, other_half]) * gate_all
    to_partner(DPART, dp_s, dp_r).start()
    part = dot(dense_in, wdd_v[:, own_half]) * gate_all

    arrive_all(RET, "ep", ret_s.at[0], ret_r)
    part = part + dot(combine_v[...], ret_r[...].reshape(n_ep * slots, half))
    to_partner(DPART, dp_s, dp_r).wait_recv()
    fin_s[...] = (part + dp_r[...]).astype(BF16).reshape(n_z, 2 * tb, half)
    scatter(FIN, "z", fin_s, fin_r)
    arrive_all(FIN, "z", fin_s.at[0], fin_r)
    mid_here = mid_r[pl.ds(2 * z, 2), :, own_half].reshape(2 * tb, half)
    out_s[...] = (mid_here.astype(F32) + total(fin_r, n_z)).astype(BF16)
    spread(OUT, "tp", out_s, out_r)
    arrive_all(OUT, "tp", out_s, out_r)
    for i in range(n_tp):
        at = slice(i // 2 * 2 * tb, (i // 2 + 1) * 2 * tb)
        mixed_out[at, i % 2 * half : (i % 2 + 1) * half] = out_r[i]

    sent_all(QP, "ep", q_s.at[0], q_r)
    sent_all(KVP, "ep", kv_s.at[0], kv_r)
    sent_all(ATT, "ep", att_s, att_r)
    sent_all(AOUT, "tp", ao_s.at[0], ao_r)
    sent_all(MID, "tp", mid_s, mid_r)
    sent_all(DISP, "ep", disp_s.at[0], disp_r)
    sent_all(DENSE, "ep", den_s.at[0], den_r)
    sent_all(DHID, "ep", dh_s, dh_r)
    sent_all(RET, "ep", ret_s.at[0], ret_r)
    sent_all(FIN, "z", fin_s.at[0], fin_r)
    sent_all(OUT, "tp", out_s, out_r)
    for k in range(n_ep - 1):
        to_partner(k, disp_r.at[0], disp_o.at[0]).wait_send()
    to_partner(WDOWN, wed_o, wed_o).wait_send()
    to_partner(HID, hid_s, hid_r).wait_send()
    to_partner(DPART, dp_s, dp_r).wait_send()


def write_out(mixed, keys, values, mixed_out, keys_out, values_out, sem):
    pairs = ((mixed, mixed_out), (keys, keys_out), (values, values_out))
    copies = [pltpu.make_async_copy(a, b, sem.at[i]) for i, (a, b) in enumerate(pairs)]
    for copy in copies:
        copy.start()
    for copy in copies:
        copy.wait()


def on_device(n_ep, n_tp, *args):
    (
        tokens,
        gain_attn,
        w_query,
        w_key,
        w_value,
        w_output,
        key_cache,
        value_cache,
        lengths,
        score_shift,
        gain_ffn,
        w_mix,
        w_dense_gate,
        w_dense_up,
        w_dense_down,
        route_group,
        route_inner,
        route_weight,
        w_exp_gate,
        w_exp_up,
        w_exp_down,
    ) = args
    batch, width = tokens.shape
    seqs, tb = batch // n_ep, batch // n_tp
    slots, half = CAP * n_ep, width // 2
    dense_cols = w_dense_gate.shape[1]
    n = max(n_ep, n_tp)
    vmem = pl.BlockSpec(memory_space=pltpu.VMEM)
    hbm = pl.BlockSpec(memory_space=pltpu.HBM)

    def like(a, skip=0):
        return pltpu.VMEM(a.shape[skip:], a.dtype)

    def both(*shape, dtype=BF16):
        return [pltpu.VMEM(shape, dtype)] * 2

    results = pl.pallas_call(
        functools.partial(layer, n_ep, n_tp, width * n_ep),
        out_shape=(
            jax.ShapeDtypeStruct((batch, width), BF16),
            jax.ShapeDtypeStruct((seqs, HD), BF16),
            jax.ShapeDtypeStruct((seqs, HD), BF16),
        ),
        in_specs=[hbm] * 21,
        out_specs=(vmem, vmem, vmem),
        scratch_shapes=[
            like(tokens), like(w_query), like(w_key), like(w_value), like(w_output),
            like(key_cache), like(value_cache),
            like(w_dense_gate), like(w_dense_up), like(w_dense_down),
            pltpu.VMEM((w_exp_gate.shape[1], 2 * w_exp_gate.shape[2]), BF16), like(w_exp_down, 1),
            pltpu.VMEM((w_exp_down.shape[1], w_exp_down.shape[2] // 2), BF16),
            like(gain_attn), pltpu.SMEM(lengths.shape, lengths.dtype),
            pltpu.SMEM(score_shift.shape, score_shift.dtype), like(gain_ffn), like(w_mix),
            like(route_group), like(route_inner.T), like(route_weight.T),
            pltpu.VMEM((1, gain_ffn.shape[0]), F32),
            pltpu.VMEM((n_ep, slots, batch), BF16),
            pltpu.VMEM((batch, n_ep * slots), BF16),
            *both(n_ep, seqs, 2 * HD),
            *both(n_ep, seqs, 2 * HD, dtype=F32),
            pltpu.VMEM((seqs, HD), BF16), pltpu.VMEM((n_ep, seqs, HD), BF16),
            *both(n_tp, tb, width),
            pltpu.VMEM((tb, width), BF16), pltpu.VMEM((n_tp, tb, width), BF16),
            *both(n_ep, slots, half), pltpu.VMEM((n_ep, slots, half), BF16),
            *both(n_ep, seqs, 2 * dense_cols + 128),
            pltpu.VMEM((seqs, dense_cols + 128), BF16),
            pltpu.VMEM((n_ep, seqs, dense_cols + 128), BF16),
            *both(slots, w_exp_gate.shape[2]),
            *both(n_ep, slots, half),
            *both(batch, half, dtype=F32),
            *both(n_tp // 2, 2 * tb, half),
            pltpu.VMEM((2 * tb, half), BF16), pltpu.VMEM((n_tp, 2 * tb, half), BF16),
            pltpu.SemaphoreType.DMA((21,)),
            pltpu.SemaphoreType.DMA((N_PHASE, n)),
            pltpu.SemaphoreType.DMA((N_PHASE, n)),
            pltpu.SemaphoreType.DMA((N_PAIR,)),
            pltpu.SemaphoreType.DMA((N_PAIR,)),
        ],
        compiler_params=pltpu.CompilerParams(
            collective_id=0, has_side_effects=True, vmem_limit_bytes=VMEM_BYTES
        ),
        name="decode_layer",
    )(
        tokens, gain_attn, w_query, w_key, w_value, w_output, key_cache, value_cache,
        lengths, score_shift, gain_ffn, w_mix,
        w_dense_gate, w_dense_up, w_dense_down,
        route_group, route_inner.T, route_weight.T,
        w_exp_gate, w_exp_up, w_exp_down,
    )
    return pl.pallas_call(
        write_out,
        out_shape=tuple(jax.ShapeDtypeStruct(r.shape, r.dtype) for r in results),
        in_specs=[vmem] * 3,
        out_specs=(hbm, hbm, hbm),
        scratch_shapes=[pltpu.SemaphoreType.DMA((3,))],
        compiler_params=pltpu.CompilerParams(vmem_limit_bytes=1024 * 1024),
        name="write_out",
    )(*results)


def solution(mesh):
    placed = (
        P(None, "ep"),
        P("ep"),
        P("ep", "tp"),
        P("ep", "tp"),
        P("ep", "tp"),
        P("tp", "ep"),
        P("ep", None, "tp"),
        P("ep", None, "tp"),
        P("ep"),
        P("tp"),
        P(),
        P("ep"),
        P("ep", "tp"),
        P("ep", "tp"),
        P("tp", "ep"),
        P(),
        P(),
        P(),
        P("ep", None, "tp"),
        P("ep", None, "tp"),
        P("ep", "tp", None),
    )
    return jax.shard_map(
        functools.partial(on_device, mesh.shape["ep"], mesh.shape["tp"]),
        mesh=mesh,
        in_specs=placed,
        out_specs=(P(None, "ep"), P("ep", "tp"), P("ep", "tp")),
        check_vma=False,
    )
```

time: 84.1 us -> 74 us (0.88)
  local copies, waits for them, and re-layouts: 7.86 us -> 2.24 us
  Pallas kernels: 74.7 us -> 70.3 us
    pallas_call x1, Pallas kernels: 74.7 us -> 69.6 us  [on_device(): pl.pallas_call(functools.partial(layer, n_ep, n_tp, width * n_ep), out_sh...]
    broadcast_in_dim x3 -> x0, local copies, waits for them, and re-layouts: 3.75 us -> none  [the longest x1 1.31 us: on_device(): gain_ffn[None, :]]
    unnamed x3 -> x6, local copies, waits for them, and re-layouts: 4.11 us -> 2.24 us
where the time goes in v2:
time: 74 us; the launch traced here: 73.8 us
  Pallas kernels  70.3 us (95%)
  local copies, waits for them, and re-layouts  2.24 us (3%)
  between operations  1.3 us (2%)
    pallas_call x1, Pallas kernels, on_device(): pl.pallas_call(functools.partial(layer, n_ep, n_tp, width * n_ep), out_sh...  69.6 us
    unnamed x6, local copies, waits for them, and re-layouts  2.24 us

profile of v2, /device:TPU:1, one launch (start us, length us, event | category | flops | bytes accessed | tf_op | source)
XLA Modules:
  0.0 73.8 jit_solution(16436199295334656827)
XLA Ops:
  1.3 69.6 %decode_layer.1 = (bf16[256,256]{1,0:T(8,128)(2,1)}, bf16[16,128]{1,0:T(8,128)(2,1)}, bf16[16,128]{1,0:T(8,128)(2,1)}) custom-call(bf16[256,256]{1,0:T(8,128)(2,1)} %tokens.1, bf16[256]{0:T(256)(128)(2,1)} %gain.1, bf16[256,128]{1,0:T(8,128)(2,1)} %wq.1, bf16[256,128]{1,0:T(8,128)(2,1)} %wk.1, bf16[256,128]{1,0:T(8,128)(2,1)} %wv.1, bf16[128,256]{1,0:T(8,128)(2,1)} %wo.1, ...), custom_call_target="tpu_custom_call" | custom-call | tf_op jit(solution)/shard_map/decode_layer/pallas_call | solution.py:535
  70.9 0.0 copy-start
  70.9 0.9 %copy-done = bf16[256,256]{1,0:T(8,128)(2,1)S(1)} copy-done((bf16[256,256]{1,0:T(8,128)(2,1)S(1)}, bf16[256,256]{1,0:T(8,128)(2,1)}, u32[]{:S(2)}) %copy-start) | copy-done | bytes 131096
  71.8 0.0 copy-start.1
  71.8 0.7 copy-done.1
  72.5 0.0 copy-start.2
  72.5 0.7 copy-done.2
  73.1 0.7 write_out.1
Async XLA Ops:
  70.9 0.9 %copy-start = (bf16[256,256]{1,0:T(8,128)(2,1)S(1)}, bf16[256,256]{1,0:T(8,128)(2,1)}, u32[]{:S(2)}) copy-start(bf16[256,256]{1,0:T(8,128)(2,1)} %get-tuple-element.6.mixed) | copy-start | bytes 393220
  71.8 0.7 copy-start.1
  72.5 0.7 copy-start.2

commit v3 on v2

--- a/solution.py
+++ b/solution.py
@@ -105,8 +105,7 @@
     wdu_v,
     wdd_v,
     wgu_v,
-    wed_v,
-    wed_o,
+    wdn_v,
     gain_v,
     len_v,
     shift_v,
@@ -146,6 +145,7 @@
     out_s,
     out_r,
     load_sem,
+    down_sem,
     send_sem,
     recv_sem,
     pair_send,
@@ -194,21 +194,23 @@
                 (wdu, wdu_v),
                 (weg.at[0], wgu_v.at[:, :ff]),
                 (weu.at[0], wgu_v.at[:, ff:]),
-                (wed.at[0], wed_v),
+                (wmix, wmix_v),
                 (wdd, wdd_v),
                 (gain, gain_v),
                 (lengths, len_v),
                 (shift, shift_v),
                 (gffn, gffn_v),
-                (wmix, wmix_v),
                 (rg, rg_v),
                 (ri, ri_v),
                 (rw, rw_v),
             )
         )
     ]
-    for load in loads:
-        load.start()
+    for i in (0, 1, 13, 2, 3, 17, 18, 19, 16, 14, 15, 11, 4, 5, 6, 7, 8, 9, 10, 12):
+        loads[i].start()
+    for i in range(n_ep):
+        at = pl.ds(pl.multiple_of(i * width + core * half, half), half)
+        pltpu.make_async_copy(wed.at[0, :, at], wdn_v.at[:ff, i * half : (i + 1) * half], down_sem).start()
 
     def copy_to(phase, axis, k, src, dst):
         return pltpu.make_async_remote_copy(
@@ -277,7 +279,7 @@
     kv_s[:, :, :HD] = dot(scaled_in, wk_v[...]).reshape(n_ep, seqs, HD)
     kv_s[:, :, HD:] = dot(scaled_in, wv_v[...]).reshape(n_ep, seqs, HD)
 
-    for i in range(14, 21):
+    for i in (14, 15, 16, 17, 18, 19, 11):
         loads[i].wait()
     gffn_row[...] = gffn_v[...].astype(F32)[None, :]
     group = rg_v[...].astype(F32)[None, :]
@@ -311,10 +313,9 @@
             (here == col0).astype(F32) + (here == col1).astype(F32)
         ).astype(BF16)
 
-    loads[11].wait()
     for i in range(n_ep):
         at = pl.ds(pl.multiple_of(i * width + (1 - core) * half, half), half)
-        to_partner(WDOWN, wed_v.at[:, at], wed_o.at[:, i * half : (i + 1) * half]).start()
+        to_partner(WDOWN, wed.at[0, :, at], wdn_v.at[ff:, i * half : (i + 1) * half]).start()
 
     arrive_all(QP, "ep", q_s.at[0], q_r)
     q_sum = total(q_r, n_ep)
@@ -369,10 +370,10 @@
 
     mid_own = mid_r[:, :, own_half].reshape(batch, half)
     mid_other = mid_r[:, :, other_half].reshape(batch, half)
-    for k, to in enumerate(ep_to):
-        disp_s[to] = dot(onehot_v[to], mid_own).astype(BF16)
-        copy_to(DISP, "ep", k, disp_s.at[to], disp_r.at[e]).start()
-    disp_r[e] = dot(onehot_v[e], mid_own).astype(BF16)
+    for i in range(0, n_ep, 4):
+        rows = onehot_v[i : i + 4].reshape(4 * slots, batch)
+        disp_s[i : i + 4] = dot(rows, mid_own).astype(BF16).reshape(4, slots, half)
+    scatter(DISP, "ep", disp_s, disp_r)
     disp_o[e] = dot(onehot_v[e], mid_other).astype(BF16)
 
     mid_f = middle.astype(F32)
@@ -395,42 +396,40 @@
     loads[9].wait()
     loads[10].wait()
 
-    def expert_part(ref, src, part, carry):
+    def expert_part(ref, sources, part, carry):
         acc, sq = carry
-        rows_f = ref[src].astype(F32)
-        at = pl.ds(pl.multiple_of(src * width + part * half, half), half)
-        scaled = (rows_f * gffn_row[:, at]).astype(BF16)
-        return acc + dot(scaled, wgu_v[at, :]), sq + rows_f * rows_f
-
+        for src in sources:
+            rows_f = ref[src].astype(F32)
+            at = pl.ds(pl.multiple_of(src * width + part * half, half), half)
+            scaled = (rows_f * gffn_row[:, at]).astype(BF16)
+            acc = acc + dot(scaled, wgu_v[at, :])
+            sq = sq + rows_f * rows_f
+        return acc, sq
+
+    def pass_on(ks):
+        for k in ks:
+            arrived(DISP, "ep", k, disp_s.at[0], disp_r)
+            to_partner(k, disp_r.at[ep_from[k]], disp_o.at[ep_from[k]]).start()
+
+    def passed_on(ks):
+        for k in ks:
+            to_partner(k, disp_r.at[ep_from[k]], disp_o.at[ep_from[k]]).wait_recv()
+
+    near = list(range(n_ep // 2 - 1, n_ep - 1))[::-1]
+    far = list(range(n_ep // 2 - 1))[::-1]
     carry = (jnp.zeros((slots, 2 * ff), F32), jnp.zeros((slots, half), F32))
-    carry = expert_part(disp_r, e, core, carry)
-    carry = expert_part(disp_o, e, 1 - core, carry)
-    nearest_first = list(reversed(range(n_ep - 1)))
-    for k in nearest_first:
-        arrived(DISP, "ep", k, disp_s.at[0], disp_r)
-        to_partner(k, disp_r.at[ep_from[k]], disp_o.at[ep_from[k]]).start()
-        carry = expert_part(disp_r, ep_from[k], core, carry)
-    for k in nearest_first:
-        to_partner(k, disp_r.at[ep_from[k]], disp_o.at[ep_from[k]]).wait_recv()
-        carry = expert_part(disp_o, ep_from[k], 1 - core, carry)
-    acc, sq = carry
+    pass_on(near)
+    carry = expert_part(disp_r, [e] + [ep_from[k] for k in near], core, carry)
+    pass_on(far)
+    passed_on(near)
+    carry = expert_part(disp_o, [e] + [ep_from[k] for k in near], 1 - core, carry)
+    carry = expert_part(disp_r, [ep_from[k] for k in far], core, carry)
+    passed_on(far)
+    acc, sq = expert_part(disp_o, [ep_from[k] for k in far], 1 - core, carry)
     inv_rows = lax.rsqrt(jnp.sum(sq, axis=1, keepdims=True) / depth_all + EPS)
     gate = acc[:, :ff] * inv_rows
     hid_s[...] = (gate / (1.0 + jnp.exp(-gate)) * (acc[:, ff:] * inv_rows)).astype(BF16)
     to_partner(HID, hid_s, hid_r).start()
-    to_partner(WDOWN, wed_o, wed_o).wait_recv()
-    to_partner(HID, hid_s, hid_r).wait_recv()
-    hidden, hidden_o = hid_s[...], hid_r[...]
-
-    def down(to):
-        at = pl.ds(pl.multiple_of(to * width + core * half, half), half)
-        at_o = pl.ds(pl.multiple_of(to * half, half), half)
-        return ((dot(hidden, wed_v[:, at]) + dot(hidden_o, wed_o[:, at_o])) * slot_weight).astype(BF16)
-
-    for k, to in enumerate(ep_to):
-        ret_s[to] = down(to)
-        copy_to(RET, "ep", k, ret_s.at[to], ret_r.at[e]).start()
-    ret_r[e] = down(e)
 
     arrive_all(DENSE, "ep", den_s.at[0], den_r)
     dense = total(den_r, n_ep)
@@ -440,18 +439,25 @@
     inv_second = lax.rsqrt(sq_sum / depth_all + EPS)
     pre = dense[:, :hidden_cols] * inv_second
     lin = dense[:, hidden_cols : 2 * hidden_cols] * inv_second
-    dh_s[:, :hidden_cols] = (pre / (1.0 + jnp.exp(-pre)) * lin).astype(BF16)
     mix_gate = 1.0 / (1.0 + jnp.exp(-mix_sum * inv_second))
-    dh_s[:, hidden_cols:] = hi_lo(mix_gate, 128).astype(BF16)
+    dh_s[...] = (pre / (1.0 + jnp.exp(-pre)) * lin * mix_gate).astype(BF16)
     spread(DHID, "ep", dh_s, dh_r)
+
+    pltpu.make_async_copy(wdn_v.at[:ff], wdn_v.at[:ff], down_sem).wait()
+    to_partner(WDOWN, wdn_v.at[ff:], wdn_v.at[ff:]).wait_recv()
+    to_partner(HID, hid_s, hid_r).wait_recv()
+    hidden = jnp.concatenate([hid_s[...], hid_r[...]], axis=1)
+    for i in range(0, n_ep, 4):
+        rows = (dot(hidden, wdn_v[:, i * half : (i + 4) * half]) * slot_weight).astype(BF16)
+        for a in range(4):
+            ret_s[i + a] = rows[:, a * half : (a + 1) * half]
+    scatter(RET, "ep", ret_s, ret_r)
     loads[12].wait()
     arrive_all(DHID, "ep", dh_s, dh_r)
-    dh_all = dh_r[...].reshape(batch, hidden_cols + 128)
-    gate_all = un_hi_lo(dh_all[:, hidden_cols:].astype(F32))
-    dense_in = dh_all[:, :hidden_cols]
-    dp_s[...] = dot(dense_in, wdd_v[:, other_half]) * gate_all
+    dense_in = dh_r[...].reshape(batch, hidden_cols)
+    dp_s[...] = dot(dense_in, wdd_v[:, other_half])
     to_partner(DPART, dp_s, dp_r).start()
-    part = dot(dense_in, wdd_v[:, own_half]) * gate_all
+    part = dot(dense_in, wdd_v[:, own_half])
 
     arrive_all(RET, "ep", ret_s.at[0], ret_r)
     part = part + dot(combine_v[...], ret_r[...].reshape(n_ep * slots, half))
@@ -480,18 +486,22 @@
     sent_all(OUT, "tp", out_s, out_r)
     for k in range(n_ep - 1):
         to_partner(k, disp_r.at[0], disp_o.at[0]).wait_send()
-    to_partner(WDOWN, wed_o, wed_o).wait_send()
+    to_partner(WDOWN, wdn_v.at[ff:], wdn_v.at[ff:]).wait_send()
     to_partner(HID, hid_s, hid_r).wait_send()
     to_partner(DPART, dp_s, dp_r).wait_send()
 
 
-def write_out(mixed, keys, values, mixed_out, keys_out, values_out, sem):
-    pairs = ((mixed, mixed_out), (keys, keys_out), (values, values_out))
-    copies = [pltpu.make_async_copy(a, b, sem.at[i]) for i, (a, b) in enumerate(pairs)]
-    for copy in copies:
-        copy.start()
-    for copy in copies:
-        copy.wait()
+def write_out(mixed, keys, values, mixed_out, keys_out, values_out, mixed_v, keys_v, values_v, sem):
+    steps = ((mixed, mixed_v, mixed_out), (keys, keys_v, keys_out), (values, values_v, values_out))
+    reads = [pltpu.make_async_copy(a, b, sem.at[i]) for i, (a, b, _) in enumerate(steps)]
+    writes = [pltpu.make_async_copy(b, c, sem.at[3 + i]) for i, (_, b, c) in enumerate(steps)]
+    for read in reads:
+        read.start()
+    for read, write in zip(reads, writes):
+        read.wait()
+        write.start()
+    for write in writes:
+        write.wait()
 
 
 def on_device(n_ep, n_tp, *args):
@@ -545,8 +555,8 @@
             like(tokens), like(w_query), like(w_key), like(w_value), like(w_output),
             like(key_cache), like(value_cache),
             like(w_dense_gate), like(w_dense_up), like(w_dense_down),
-            pltpu.VMEM((w_exp_gate.shape[1], 2 * w_exp_gate.shape[2]), BF16), like(w_exp_down, 1),
-            pltpu.VMEM((w_exp_down.shape[1], w_exp_down.shape[2] // 2), BF16),
+            pltpu.VMEM((w_exp_gate.shape[1], 2 * w_exp_gate.shape[2]), BF16),
+            pltpu.VMEM((2 * w_exp_down.shape[1], w_exp_down.shape[2] // 2), BF16),
             like(gain_attn), pltpu.SMEM(lengths.shape, lengths.dtype),
             pltpu.SMEM(score_shift.shape, score_shift.dtype), like(gain_ffn), like(w_mix),
             like(route_group), like(route_inner.T), like(route_weight.T),
@@ -560,14 +570,15 @@
             pltpu.VMEM((tb, width), BF16), pltpu.VMEM((n_tp, tb, width), BF16),
             *both(n_ep, slots, half), pltpu.VMEM((n_ep, slots, half), BF16),
             *both(n_ep, seqs, 2 * dense_cols + 128),
-            pltpu.VMEM((seqs, dense_cols + 128), BF16),
-            pltpu.VMEM((n_ep, seqs, dense_cols + 128), BF16),
+            pltpu.VMEM((seqs, dense_cols), BF16),
+            pltpu.VMEM((n_ep, seqs, dense_cols), BF16),
             *both(slots, w_exp_gate.shape[2]),
             *both(n_ep, slots, half),
             *both(batch, half, dtype=F32),
             *both(n_tp // 2, 2 * tb, half),
             pltpu.VMEM((2 * tb, half), BF16), pltpu.VMEM((n_tp, 2 * tb, half), BF16),
-            pltpu.SemaphoreType.DMA((21,)),
+            pltpu.SemaphoreType.DMA((20,)),
+            pltpu.SemaphoreType.DMA,
             pltpu.SemaphoreType.DMA((N_PHASE, n)),
             pltpu.SemaphoreType.DMA((N_PHASE, n)),
             pltpu.SemaphoreType.DMA((N_PAIR,)),
@@ -587,10 +598,10 @@
     return pl.pallas_call(
         write_out,
         out_shape=tuple(jax.ShapeDtypeStruct(r.shape, r.dtype) for r in results),
-        in_specs=[vmem] * 3,
+        in_specs=[hbm] * 3,
         out_specs=(hbm, hbm, hbm),
-        scratch_shapes=[pltpu.SemaphoreType.DMA((3,))],
-        compiler_params=pltpu.CompilerParams(vmem_limit_bytes=1024 * 1024),
+        scratch_shapes=[*(pltpu.VMEM(r.shape, r.dtype) for r in results), pltpu.SemaphoreType.DMA((6,))],
+        compiler_params=pltpu.CompilerParams(vmem_limit_bytes=VMEM_BYTES),
         name="write_out",
     )(*results)
 

time: 74 us -> 67.1 us (0.907)
  Pallas kernels: 70.3 us -> 65.7 us
  local copies, waits for them, and re-layouts: 2.24 us -> 0 us
    pallas_call x1, Pallas kernels: 69.6 us -> 64.1 us  [on_device(): pl.pallas_call(functools.partial(layer, n_ep, n_tp, width * n_ep), out_sh...]
    unnamed x6 -> x0, local copies, waits for them, and re-layouts: 2.24 us -> none
    pallas_call x1, Pallas kernels: 0.68 us -> 1.62 us  [on_device(): pl.pallas_call(write_out, out_shape=tuple((jax.ShapeDtypeStruct(r.shape,...]
where the time goes in v3:
time: 67.1 us; the launch traced here: 67 us
  Pallas kernels  65.7 us (98%)
  between operations  1.29 us (2%)
    pallas_call x1, Pallas kernels, on_device(): pl.pallas_call(functools.partial(layer, n_ep, n_tp, width * n_ep), out_sh...  64.1 us
    pallas_call x1, Pallas kernels, on_device(): pl.pallas_call(write_out, out_shape=tuple((jax.ShapeDtypeStruct(r.shape,...  1.62 us

profile of v3, /device:TPU:1, one launch (start us, length us, event | category | flops | bytes accessed | tf_op | source)
XLA Modules:
  0.0 67.0 jit_solution(17728377718381358326)
XLA Ops:
  1.3 64.1 %decode_layer.1 = (bf16[256,256]{1,0:T(8,128)(2,1)}, bf16[16,128]{1,0:T(8,128)(2,1)}, bf16[16,128]{1,0:T(8,128)(2,1)}) custom-call(bf16[256,256]{1,0:T(8,128)(2,1)} %tokens.1, bf16[256]{0:T(256)(128)(2,1)} %gain.1, bf16[256,128]{1,0:T(8,128)(2,1)} %wq.1, bf16[256,128]{1,0:T(8,128)(2,1)} %wk.1, bf16[256,128]{1,0:T(8,128)(2,1)} %wv.1, bf16[128,256]{1,0:T(8,128)(2,1)} %wo.1, ...), custom_call_target="tpu_custom_call" | custom-call | tf_op jit(solution)/shard_map/decode_layer/pallas_call | solution.py:545
  65.4 1.6 %write_out.1 = (bf16[256,256]{1,0:T(8,128)(2,1)}, bf16[16,128]{1,0:T(8,128)(2,1)}, bf16[16,128]{1,0:T(8,128)(2,1)}) custom-call(bf16[256,256]{1,0:T(8,128)(2,1)} %get-tuple-element.6.mixed, bf16[16,128]{1,0:T(8,128)(2,1)} %get-tuple-element.7.keys, bf16[16,128]{1,0:T(8,128)(2,1)} %get-tuple-element.8.values), custom_call_target="tpu_custom_call" | custom-call | tf_op jit(solution)/shard_map/write_out/pallas_call | solution.py:598
